TPU v7x, 32 devices: a whole 2x2x4 slice. The times are simulated.
32 devices in a mesh: grp: 2 (over y), tp: 4 (over z), dp: 4 (over x, core).
Axes of the slice: x: 2, y: 2, z: 4, core: 2. Of those that a mesh axis runs over, the one named last changes fastest.
Arguments:
- hidden_in: bfloat16 [96, 4096], P(('grp', 'tp'), 'dp'), parts along dimension 0, may hold values from -40 to 40
- input_norm_gain: float32 [2, 4096], P(None, 'dp'), may hold values from 0.1 to 1.9
- w_query: bfloat16 [2, 4096, 2048], P(None, 'dp', 'tp'), may hold values from -0.09375 to 0.09375
- w_key: bfloat16 [2, 4096, 2048], P(None, 'dp', 'tp'), may hold values from -0.09375 to 0.09375
- w_decay: bfloat16 [2, 4096, 2048], P(None, 'dp', 'tp'), may hold values from -0.375 to 0.375
- w_value: bfloat16 [2, 4096, 4096], P(None, 'dp', 'tp'), may hold values from -0.09375 to 0.09375
- w_gate: bfloat16 [2, 4096, 4096], P(None, 'dp', 'tp'), may hold values from -0.09375 to 0.09375
- out_gain: float32 [2, 4096], P(None, 'tp'), may hold values from 0.1 to 1.9
- w_out: bfloat16 [2, 4096, 4096], P(None, 'tp', 'dp'), may hold values from -0.09375 to 0.09375
- decay_offset: float32 [2, 96, 2048], P(None, ('grp', 'dp'), 'tp'), parts along dimension 1, may hold values from -0.7 to 0
- state: float32 [2, 96, 32, 64, 128], P(None, ('grp', 'dp'), 'tp'), parts along dimension 1, may hold values from -3 to 3
Outputs:
- hidden_out: bfloat16 [96, 4096], P(('grp', 'tp'), 'dp'), parts along dimension 0
- new_state: float32 [2, 96, 32, 64, 128], P(None, ('grp', 'dp'), 'tp'), parts along dimension 1
There are 2 independent parts, one for each index of `grp`. A program takes and returns all parts, laid end to end along the dimension named above; an argument that names none is the same for every part. Nothing has to cross between parts.
All inputs are finite; a program needn't handle non-finite values.
Results may differ from a plain program's by a relative error of at most 0.017.
Values may be sent and summed in bfloat16 or wider, within the bound.
A program may use at most 64 MiB of HBM per device.

v0:
```python
import functools

import jax
import jax.numpy as jnp
from jax import lax
from jax.experimental import pallas as pl
from jax.experimental.pallas import tpu as pltpu
from jax.sharding import PartitionSpec as P

EPSILON = 1e-06
SOFTNESS = 16.0
F32 = jnp.float32
BF16 = jnp.bfloat16


def pack(block, rows):
    if block.shape[0] != 16 or rows > 12 or block.shape[1] % 256:
        return block
    half = block.shape[1] // 2
    tail = jnp.concatenate([block[8:12, :half], block[8:12, half:]], axis=0)
    return jnp.concatenate([block[:8], tail], axis=1)


def unpack(block, rows, columns):
    if block.shape[1] == columns:
        return block
    tail = jnp.concatenate([block[:4, columns:], block[4:, columns:]], axis=1)
    return jnp.concatenate([block[:, :columns], tail, jnp.zeros_like(tail)], axis=0)


def packed_shape(pad, rows, columns):
    if pad != 16 or rows > 12 or columns % 256:
        return pad, columns
    return 8, columns // 2 * 3


def block_kernel(
    n_tp, n_dp, d_model, head_key, value_channels, piece, mix_piece,
    hidden_ref, gain_ref, out_gain_ref, offset_ref,
    wq_hbm, wk_hbm, wd_hbm, wv_hbm, wg_hbm, wo_hbm, state_hbm,
    hidden_out_ref, new_state_ref,
    wq, wk, wd, wv, wg, wo, state,
    current, gathered, part_send, part_recv, sq_send, sq_recv,
    turned, products, value_buf, gate_buf, decay_buf, readout,
    gated_all, mix_send, mix_recv,
    load_sem, gather_sems, part_sems, sq_sems, gated_sems, mix_sems,
):
    layers, rows, heads = state.shape[0], state.shape[1], state.shape[2]
    pad = current.shape[1]
    mix_pieces = mix_send.shape[1]
    key_cols = heads * head_key
    value_cols = heads * value_channels
    tp = lax.axis_index("tp")
    dp = lax.axis_index("dp")

    sources = (wq_hbm, wk_hbm, wd_hbm, wv_hbm, wg_hbm, wo_hbm, state_hbm)
    targets = (wq, wk, wd, wv, wg, wo, state)

    def load(index, layer):
        return pltpu.make_async_copy(
            sources[index].at[layer], targets[index].at[layer], load_sem.at[index, layer]
        )

    for layer in range(layers):
        for index in (0, 1, 2, 3, 4, 6, 5):
            load(index, layer).start()

    barrier = pltpu.get_barrier_semaphore()
    for j in range(1, n_tp):
        pl.semaphore_signal(
            barrier, inc=1, device_id={"tp": lax.rem(tp + j, n_tp)},
            device_id_type=pl.DeviceIdType.MESH,
        )
    for j in range(1, n_dp):
        pl.semaphore_signal(
            barrier, inc=1, device_id={"dp": lax.rem(dp + j, n_dp)},
            device_id_type=pl.DeviceIdType.MESH,
        )
    current[0, pl.ds(0, rows), :] = hidden_ref[...]
    for layer in range(layers):
        readout[layer] = jnp.zeros_like(readout[layer])
    pl.semaphore_wait(barrier, n_tp + n_dp - 2)

    def remote(src, dst, sems, index, axis, target):
        return pltpu.make_async_remote_copy(
            src_ref=src, dst_ref=dst,
            send_sem=sems.at[(0,) + index], recv_sem=sems.at[(1,) + index],
            device_id={axis: target}, device_id_type=pl.DeviceIdType.MESH,
        )

    pending = []

    def send_features(layer, p):
        block = current[layer, :, pl.ds(p * mix_piece, mix_piece)].astype(F32)
        gathered[layer, p, tp] = pack(block, rows).astype(BF16)
        sent = []
        for j in range(1, n_tp):
            copy = remote(
                gathered.at[layer, p, tp], gathered.at[layer, p, tp], gather_sems,
                (layer, p, j - 1), "tp", lax.rem(tp + j, n_tp),
            )
            copy.start()
            sent.append(copy)
        return sent

    feature_copies = []
    for p in range(mix_pieces):
        feature_copies += send_features(0, p)

    for layer in range(layers):
        copies = feature_copies
        feature_copies = []
        for copy in copies:
            copy.wait_recv()
        pending += copies
        widened = jnp.concatenate(
            [
                jnp.concatenate(
                    [
                        unpack(gathered[layer, p, s].astype(F32), rows, mix_piece)
                        for p in range(mix_pieces)
                    ],
                    axis=1,
                )
                for s in range(n_tp)
            ],
            axis=0,
        )
        scaled = (widened * gain_ref[layer, :][None, :]).astype(BF16)
        squares = jnp.sum(widened * widened, axis=1, keepdims=True)
        sq_send[layer] = jnp.broadcast_to(squares, (n_tp * pad, 128)).reshape(n_tp, pad, 128)
        sq_copies = []
        for j in range(1, n_dp):
            to = lax.rem(dp + j, n_dp)
            copy = remote(
                sq_send.at[layer, to], sq_recv.at[layer, j - 1], sq_sems, (layer, j - 1), "dp", to
            )
            copy.start()
            sq_copies.append(copy)

        part_copies = []
        p = 0
        for index, matrix in enumerate((wq, wk, wd, wv, wg)):
            load(index, layer).wait()
            for start in range(0, matrix.shape[2], piece):
                result = jnp.dot(
                    scaled, matrix[layer, :, pl.ds(start, piece)], preferred_element_type=F32
                )
                for s in range(n_dp):
                    block = result[s * pad : (s + 1) * pad]
                    part_send[layer, p, s] = pack(block, rows).astype(BF16)
                for j in range(1, n_dp):
                    to = lax.rem(dp + j, n_dp)
                    copy = remote(
                        part_send.at[layer, p, to], part_recv.at[layer, p, j - 1],
                        part_sems, (layer, p, j - 1), "dp", to,
                    )
                    copy.start()
                    part_copies.append(copy)
                p += 1
        pending += sq_copies + part_copies

        for copy in sq_copies:
            copy.wait_recv()
        total_squares = sq_send[layer, dp]
        for j in range(1, n_dp):
            total_squares = total_squares + sq_recv[layer, j - 1]
        inverse = lax.rsqrt(total_squares / d_model + EPSILON)[:, :1]

        def projected(p):
            for j in range(1, n_dp):
                part_copies[p * (n_dp - 1) + j - 1].wait_recv()
            total = part_send[layer, p, dp].astype(F32)
            for j in range(1, n_dp):
                total = total + part_recv[layer, p, j - 1].astype(F32)
            return unpack(total, rows, piece) * inverse

        def projected_range(first, columns):
            got = [projected(first + i) for i in range(columns // piece)]
            return got[0] if len(got) == 1 else jnp.concatenate(got, axis=1)

        per_key = key_cols // piece
        per_value = value_cols // piece
        query = projected_range(0, key_cols)
        key = projected_range(per_key, key_cols) * head_key ** (-0.5)
        logits = projected_range(2 * per_key, key_cols)
        log_sigmoid = jnp.minimum(logits, 0.0) - jnp.log(1.0 + jnp.exp(-jnp.abs(logits)))
        decay_buf[layer, pl.ds(0, rows), :] = (
            log_sigmoid[:rows] / SOFTNESS + offset_ref[:, layer, :]
        )
        decay = jnp.exp(decay_buf[layer])
        stacked = jnp.concatenate(
            [query * decay, key, decay, jnp.zeros((128 - 3 * pad, key_cols), F32)], axis=0
        )
        turned[layer] = stacked.T.reshape(heads, head_key, 128)
        both = query * key
        for h in range(heads):
            own = both[:, h * head_key : (h + 1) * head_key]
            products[layer, h] = jnp.broadcast_to(
                jnp.sum(own, axis=1, keepdims=True), (pad, 128)
            )
        load(6, layer).wait()

        def read_head(h, _):
            columns = turned[layer, h]
            for b in range(rows):
                factor = jnp.broadcast_to(columns[:, b : b + 1], (head_key, value_channels))
                readout[layer, h, pl.ds(b, 1), :] = jnp.sum(
                    factor * state[layer, b, h], axis=0, keepdims=True
                )
            return 0

        lax.fori_loop(0, heads, read_head, 0)

        value_buf[layer] = projected_range(3 * per_key, value_cols)
        gate_buf[layer] = projected_range(3 * per_key + per_value, value_cols)
        gated_heads = []
        for h in range(heads):
            span = slice(h * value_channels, (h + 1) * value_channels)
            got = readout[layer, h] + products[layer, h] * value_buf[layer, :, span]
            gate = gate_buf[layer, :, span]
            normed = got * lax.rsqrt(jnp.mean(got * got, axis=1, keepdims=True) + EPSILON)
            normed = normed * out_gain_ref[layer, span][None, :]
            gated_heads.append(normed * (gate / (1.0 + jnp.exp(-gate))))
        gated_all[layer, dp] = pack(jnp.concatenate(gated_heads, axis=1), rows).astype(BF16)

        copies = []
        for j in range(1, n_dp):
            copy = remote(
                gated_all.at[layer, dp], gated_all.at[layer, dp], gated_sems, (layer, j - 1),
                "dp", lax.rem(dp + j, n_dp),
            )
            copy.start()
            copies.append(copy)

        def renew_head(h, _):
            columns = turned[layer, h]
            values = value_buf[layer, :, pl.ds(pl.multiple_of(h * value_channels, value_channels), value_channels)]
            for b in range(rows):
                shape = (head_key, value_channels)
                keep = jnp.broadcast_to(columns[:, 2 * pad + b : 2 * pad + b + 1], shape)
                add = jnp.broadcast_to(columns[:, pad + b : pad + b + 1], shape)
                new_state_ref[layer, b, h] = keep * state[layer, b, h] + add * values[b : b + 1]
            return 0

        lax.fori_loop(0, heads, renew_head, 0)

        load(5, layer).wait()
        for copy in copies:
            copy.wait_recv()
        pending += copies

        gated = jnp.concatenate(
            [
                unpack(gated_all[layer, s].astype(F32), rows, value_cols).astype(BF16)
                for s in range(n_dp)
            ],
            axis=0,
        )
        mix_copies = []
        for p in range(mix_pieces):
            result = jnp.dot(
                gated, wo[layer, :, pl.ds(p * mix_piece, mix_piece)], preferred_element_type=F32
            )
            for s in range(n_tp):
                block = result[s * pad : (s + 1) * pad]
                mix_send[layer, p, s] = pack(block, rows).astype(BF16)
            for j in range(1, n_tp):
                to = lax.rem(tp + j, n_tp)
                copy = remote(
                    mix_send.at[layer, p, to], mix_recv.at[layer, p, j - 1],
                    mix_sems, (layer, p, j - 1), "tp", to,
                )
                copy.start()
                mix_copies.append(copy)
        pending += mix_copies
        for p in range(mix_pieces):
            span = slice(p * mix_piece, (p + 1) * mix_piece)
            for j in range(1, n_tp):
                mix_copies[p * (n_tp - 1) + j - 1].wait_recv()
            total = mix_send[layer, p, tp].astype(F32)
            for j in range(1, n_tp):
                total = total + mix_recv[layer, p, j - 1].astype(F32)
            total = unpack(total, rows, mix_piece)
            result = (current[layer, :, span].astype(F32) + total).astype(BF16)
            if layer + 1 < layers:
                current[layer + 1, :, span] = result
                feature_copies += send_features(layer + 1, p)
            else:
                hidden_out_ref[:, span] = result[:rows]

    for copy in pending:
        copy.wait_send()


def fused(
    n_tp, n_dp, hidden_in, input_norm_gain, w_query, w_key, w_decay, w_value, w_gate,
    out_gain, w_out, decay_offset, state,
):
    layers, rows, heads, head_key, value_channels = state.shape
    width = hidden_in.shape[1]
    pad = -(-rows // 16) * 16
    key_cols, value_cols = w_query.shape[2], w_value.shape[2]
    piece = min(512, key_cols)
    pieces = (3 * key_cols + 2 * value_cols) // piece
    mix_piece = min(512, width)
    mix_pieces = width // mix_piece
    part_shape = packed_shape(pad, rows, piece)
    mix_shape = packed_shape(pad, rows, mix_piece)
    vmem = pl.BlockSpec(memory_space=pltpu.VMEM)
    hbm = pl.BlockSpec(memory_space=pl.ANY)
    return pl.pallas_call(
        functools.partial(
            block_kernel, n_tp, n_dp, width * n_dp, head_key, value_channels,
            piece, mix_piece,
        ),
        out_shape=(
            jax.ShapeDtypeStruct(hidden_in.shape, BF16),
            pltpu.VMEM(state.shape, F32),
        ),
        in_specs=[vmem] * 4 + [hbm] * 7,
        out_specs=(vmem, vmem),
        scratch_shapes=[
            pltpu.VMEM(w_query.shape, BF16),
            pltpu.VMEM(w_key.shape, BF16),
            pltpu.VMEM(w_decay.shape, BF16),
            pltpu.VMEM(w_value.shape, BF16),
            pltpu.VMEM(w_gate.shape, BF16),
            pltpu.VMEM(w_out.shape, BF16),
            pltpu.VMEM(state.shape, F32),
            pltpu.VMEM((layers, pad, width), BF16),
            pltpu.VMEM((layers, mix_pieces, n_tp) + mix_shape, BF16),
            pltpu.VMEM((layers, pieces, n_dp) + part_shape, BF16),
            pltpu.VMEM((layers, pieces, n_dp - 1) + part_shape, BF16),
            pltpu.VMEM((layers, n_dp, pad, 128), F32),
            pltpu.VMEM((layers, n_dp - 1, pad, 128), F32),
            pltpu.VMEM((layers, heads, head_key, 128), F32),
            pltpu.VMEM((layers, heads, pad, 128), F32),
            pltpu.VMEM((layers, pad, value_cols), F32),
            pltpu.VMEM((layers, pad, value_cols), F32),
            pltpu.VMEM((layers, pad, key_cols), F32),
            pltpu.VMEM((layers, heads, pad, value_channels), F32),
            pltpu.VMEM((layers, n_dp) + packed_shape(pad, rows, value_cols), BF16),
            pltpu.VMEM((layers, mix_pieces, n_tp) + mix_shape, BF16),
            pltpu.VMEM((layers, mix_pieces, n_tp - 1) + mix_shape, BF16),
            pltpu.SemaphoreType.DMA((7, layers)),
            pltpu.SemaphoreType.DMA((2, layers, mix_pieces, n_tp - 1)),
            pltpu.SemaphoreType.DMA((2, layers, pieces, n_dp - 1)),
            pltpu.SemaphoreType.DMA((2, layers, n_dp - 1)),
            pltpu.SemaphoreType.DMA((2, layers, n_dp - 1)),
            pltpu.SemaphoreType.DMA((2, layers, mix_pieces, n_tp - 1)),
        ],
        compiler_params=pltpu.CompilerParams(
            collective_id=0, has_side_effects=True, vmem_limit_bytes=48 * 1024 * 1024
        ),
    )(
        hidden_in, input_norm_gain, out_gain, decay_offset.transpose(1, 0, 2),
        w_query, w_key, w_decay, w_value, w_gate, w_out, state,
    )


def plain(
    hidden_in, input_norm_gain, w_query, w_key, w_decay, w_value, w_gate,
    out_gain, w_out, decay_offset, state,
):
    layers, rows, heads, head_key, value_channels = state.shape
    key_cols, value_cols = w_query.shape[2], w_value.shape[2]
    d_model = hidden_in.shape[1] * lax.axis_size("dp")
    first = lax.axis_index("dp") * rows
    current, states = hidden_in, []
    for layer in range(layers):
        widened = lax.all_gather(current, "tp", axis=0, tiled=True).astype(F32)
        squares = lax.psum(jnp.sum(widened * widened, axis=1), "dp")
        scaled = (widened * input_norm_gain[layer][None, :]).astype(BF16)
        partial = jnp.concatenate(
            [
                jnp.dot(scaled, matrix[layer], preferred_element_type=F32)
                for matrix in (w_query, w_key, w_decay, w_value, w_gate)
            ],
            axis=1,
        ).astype(BF16)
        summed = lax.psum_scatter(partial, "dp", scatter_dimension=0, tiled=True).astype(F32)
        own = lax.dynamic_slice_in_dim(squares, first, rows)
        projected = summed * lax.rsqrt(own / d_model + EPSILON)[:, None]
        query, key, logits, value, gate = jnp.split(
            projected,
            [key_cols, 2 * key_cols, 3 * key_cols, 3 * key_cols + value_cols],
            axis=1,
        )
        decay = jnp.exp(jax.nn.log_sigmoid(logits) / SOFTNESS + decay_offset[layer])
        per_key, per_value = (rows, heads, head_key), (rows, heads, value_channels)
        fresh = (
            decay.reshape(per_key)[..., None] * state[layer]
            + (key * head_key ** (-0.5)).reshape(per_key)[..., None]
            * value.reshape(per_value)[:, :, None, :]
        )
        got = jnp.sum(query.reshape(per_key)[..., None] * fresh, axis=2)
        got = got * lax.rsqrt(jnp.mean(got * got, axis=2, keepdims=True) + EPSILON)
        got = got * out_gain[layer].reshape(heads, value_channels)[None]
        gated = (got * jax.nn.silu(gate.reshape(per_value))).reshape(rows, value_cols).astype(BF16)
        mixed = jnp.dot(
            lax.all_gather(gated, "dp", axis=0, tiled=True), w_out[layer],
            preferred_element_type=F32,
        ).astype(BF16)
        mine = lax.psum_scatter(mixed, "tp", scatter_dimension=0, tiled=True).astype(F32)
        current = (current.astype(F32) + mine).astype(BF16)
        states.append(fresh)
    return current, jnp.stack(states)


def solution(mesh):
    n_tp, n_dp = mesh.shape["tp"], mesh.shape["dp"]

    def per_device(hidden_in, *rest):
        state = rest[-1]
        aligned = rest[1].shape[2] % 128 == 0 and hidden_in.shape[1] % 128 == 0
        if n_tp > 1 and n_tp == n_dp and aligned and 3 * state.shape[1] <= 96:
            return fused(n_tp, n_dp, hidden_in, *rest)
        return plain(hidden_in, *rest)

    return jax.shard_map(
        per_device,
        mesh=mesh,
        in_specs=(
            P(("grp", "tp"), "dp"),
            P(None, "dp"),
            P(None, "dp", "tp"),
            P(None, "dp", "tp"),
            P(None, "dp", "tp"),
            P(None, "dp", "tp"),
            P(None, "dp", "tp"),
            P(None, "tp"),
            P(None, "tp", "dp"),
            P(None, ("grp", "dp"), "tp"),
            P(None, ("grp", "dp"), "tp", None, None),
        ),
        out_specs=(P(("grp", "tp"), "dp"), P(None, ("grp", "dp"), "tp", None, None)),
        check_vma=False,
    )
```

profile of v0, /device:TPU:0, one launch (start us, length us, event | category | flops | bytes accessed | tf_op | source)
XLA Modules:
  0.0 46.8 jit_solution(16544122373267611901)
XLA Ops:
  0.6 42.8 %shard_map.122 = (bf16[12,1024]{1,0:T(8,128)(2,1)}, f32[2,12,8,64,128]{4,3,2,1,0:T(8,128)S(1)}) custom-call(bf16[12,1024]{1,0:T(8,128)(2,1)} %hidden_ref.1, f32[2,1024]{1,0:T(2,128)} %gain_ref.1, f32[2,1024]{1,0:T(2,128)} %out_gain_ref.1, f32[12,2,512]{2,1,0:T(2,128)} %bitcast.1, bf16[2,1024,512]{2,1,0:T(8,128)(2,1)} %wq_hbm.1, ...), custom_call_target="tpu_custom_call" | custom-call | tf_op jit(solution)/shard_map/pallas_call | solution.py:312
  43.5 0.0 copy-start
  43.5 2.7 %copy.15 = f32[2,12,8,64,128]{4,3,2,1,0:T(8,128)} copy(f32[2,12,8,64,128]{4,3,2,1,0:T(8,128)S(1)} %get-tuple-element.3) | data formatting | bytes 12582912
  46.2 0.0 copy-done
  46.2 0.6 %copy.16 = bf16[12,1024]{1,0:T(8,128)(2,1)} copy(bf16[12,1024]{1,0:T(8,128)(2,1)S(1)} %copy-done) | data formatting | bytes 49152
Async XLA Ops:
  43.5 2.7 %copy-start = (bf16[12,1024]{1,0:T(8,128)(2,1)S(1)}, bf16[12,1024]{1,0:T(8,128)(2,1)}, u32[]{:S(2)}) copy-start(bf16[12,1024]{1,0:T(8,128)(2,1)} %get-tuple-element.6) | copy-start | bytes 73732
where the time goes:
time: 47 us; the launch traced here: 46.8 us
  Pallas kernels  42.8 us (91%)
  local copies, waits for them, and re-layouts  3.32 us (7%)
  between operations  0.65 us (1%)
    pallas_call x1, Pallas kernels, fused(): pl.pallas_call(functools.partial(block_kernel, n_tp, n_dp, width * n_dp,...  42.8 us
    unnamed x4, local copies, waits for them, and re-layouts  3.32 us

commit v1 on v0

v1 whole, which is shorter than its diff:
```python
import functools

import jax
import jax.numpy as jnp
from jax import lax
from jax.experimental import pallas as pl
from jax.experimental.pallas import tpu as pltpu
from jax.sharding import PartitionSpec as P

EPSILON = 1e-06
SOFTNESS = 16.0
F32 = jnp.float32
BF16 = jnp.bfloat16


def swap(tiles):
    return pltpu.roll(tiles, 4, 0)


def first_half(shape):
    return lax.broadcasted_iota(jnp.int32, shape, 0) < 4


def fold(upper, lower, second):
    even = jnp.concatenate([lower[:, :128], lower[:, 256:384]], axis=1)
    odd = jnp.concatenate([lower[:, 128:256], lower[:, 384:]], axis=1)
    top = first_half(even.shape)
    first_form = jnp.where(top, even, swap(odd))
    second_form = jnp.where(top, swap(even), odd)
    if isinstance(second, int):
        folded = second_form if second else first_form
    else:
        folded = jnp.where(second == 1, second_form, first_form)
    return jnp.concatenate(
        [
            jnp.concatenate([upper[:, :256], folded[:, :128]], axis=1),
            jnp.concatenate([upper[:, 256:], folded[:, 128:]], axis=1),
        ],
        axis=0,
    )


def unfold(block):
    upper = jnp.concatenate([block[:8, :256], block[8:, :256]], axis=1)
    left, right = block[:8, 256:], block[8:, 256:]
    lower = jnp.concatenate([left, swap(left), right, swap(right)], axis=1)
    return upper, lower


def unfold_rows(block):
    upper, lower = unfold(block)
    return jnp.concatenate([upper, jnp.where(first_half(lower.shape), lower, 0.0)], axis=0)


def stack_groups(blocks):
    rows = []
    for core in range(2):
        one, two = blocks[core], blocks[2 + core]
        upper_one = jnp.concatenate([one[:8, :256], one[8:, :256]], axis=1)
        upper_two = jnp.concatenate([two[:8, :256], two[8:, :256]], axis=1)
        lower = []
        for half in range(2):
            a, b = one[8 * half : 8 * half + 8, 256:], two[8 * half : 8 * half + 8, 256:]
            top = first_half(a.shape)
            lower += [jnp.where(top, a, swap(b)), jnp.where(top, swap(a), b)]
        rows += [upper_one, upper_two, jnp.concatenate(lower, axis=1)]
    return jnp.concatenate(rows, axis=0)


def group_of(stacked, s):
    chip, core = divmod(s, 2)
    base = 24 * core
    upper = stacked[base + 8 * chip : base + 8 * chip + 8]
    return fold(upper, stacked[base + 16 : base + 24], chip)


def block_kernel(
    n_tp, n_dp, d_model, head_key, value_channels, piece,
    hidden_hbm, gain_hbm, out_gain_hbm, offset_hbm,
    wq_hbm, wk_hbm, wd_hbm, wv_hbm, wg_hbm, wo_hbm, state_hbm,
    hidden_out_ref, new_state_ref,
    hidden, gain, out_gain, offset, proj, wo, state,
    gathered, product, partial, near, own, cross, far,
    sq_part, sq_near, sq_cross, sq_far,
    expand, values, fresh_columns, readout,
    gated_all, mix_part, mix_send, mix_recv,
    small_sem, proj_sem, wo_sem, state_sem,
    gather_recv, near_recv, far_recv, sq_recv, gated_recv, mix_recv_sem, send_sem,
):
    layers, rows, heads = state.shape[0], state.shape[1], state.shape[2]
    pad = 16
    mix_pieces = mix_send.shape[1]
    pieces = proj.shape[1]
    key_cols = heads * head_key
    value_cols = heads * value_channels
    halves = value_cols // piece
    half_heads = heads // halves
    tp = lax.axis_index("tp")
    dp = lax.axis_index("dp")
    chip, core = dp // 2, lax.rem(dp, 2)
    other_core = 1 - core
    other_chip = 1 - chip
    partner = 2 * chip + other_core
    across = 2 * other_chip + core
    mesh_id = pl.DeviceIdType.MESH

    barrier = pltpu.get_barrier_semaphore()
    for j in range(1, n_tp):
        pl.semaphore_signal(
            barrier, inc=1, device_id={"tp": lax.rem(tp + j, n_tp)}, device_id_type=mesh_id
        )
    for j in range(1, n_dp):
        pl.semaphore_signal(
            barrier, inc=1, device_id={"dp": lax.rem(dp + j, n_dp)}, device_id_type=mesh_id
        )

    small = [
        pltpu.make_async_copy(source, target, small_sem.at[index])
        for index, (source, target) in enumerate(
            ((hidden_hbm, hidden), (gain_hbm, gain), (out_gain_hbm, out_gain), (offset_hbm, offset))
        )
    ]

    def load_proj(layer, i):
        if i < 3:
            source = (wq_hbm, wk_hbm, wd_hbm)[i].at[layer]
        else:
            half, which = divmod(i - 3, 2)
            source = (wv_hbm, wg_hbm)[which].at[layer, :, pl.ds(half * piece, piece)]
        return pltpu.make_async_copy(source, proj.at[layer, i], proj_sem.at[layer, i])

    def load_wo(layer):
        return pltpu.make_async_copy(wo_hbm.at[layer], wo.at[layer], wo_sem.at[layer])

    def load_state(layer):
        return pltpu.make_async_copy(state_hbm.at[layer], state.at[layer], state_sem.at[layer])

    for copy in small:
        copy.start()

    row_of = lax.broadcasted_iota(jnp.int32, (4 * pad, 2 * value_channels), 0)
    lane_of = lax.broadcasted_iota(jnp.int32, (4 * pad, 2 * value_channels), 1)
    for second in range(2):
        for pair in range(rows // 2):
            picked = pair * 2 + lane_of // value_channels
            inside = (row_of >= second * 2 * pad) & (row_of < (second + 1) * 2 * pad)
            hit = inside & (lax.rem(row_of, pad) == picked)
            expand[second, pair] = jnp.where(hit, 1.0, 0.0).astype(BF16)

    for copy in small:
        copy.wait()
    for layer in range(layers):
        for i in range(pieces):
            load_proj(layer, i).start()
        load_state(layer).start()
        load_wo(layer).start()

    upper = hidden[pl.ds(0, 8), :].astype(F32)
    lower = hidden[pl.ds(8, 4), :].astype(F32)
    lower = jnp.concatenate([lower, lower], axis=0)
    for p in range(mix_pieces):
        span = slice(p * piece, (p + 1) * piece)
        gathered[0, p, tp] = fold(upper[:, span], lower[:, span], 0).astype(BF16)
    pl.semaphore_wait(barrier, n_tp + n_dp - 2)

    def remote(src, dst, send, recv, axis, target):
        copy = pltpu.make_async_remote_copy(
            src_ref=src, dst_ref=dst, send_sem=send, recv_sem=recv,
            device_id={axis: target}, device_id_type=mesh_id,
        )
        copy.start()

    def await_bytes(ref, sem):
        pltpu.make_async_copy(ref, ref, sem).wait()

    above = tp // (n_tp // 2)

    def tp_step(j):
        return j + above * (n_tp - 2 * j)

    def send_features(layer, p):
        for j in range(n_tp - 1, 0, -1):
            remote(
                gathered.at[layer, p, tp], gathered.at[layer, p, tp],
                send_sem.at[layer, 0], gather_recv.at[layer, p],
                "tp", lax.rem(tp + tp_step(j), n_tp),
            )

    def split(block):
        high = block.astype(BF16).astype(F32)
        return [high, block - high]

    def columns_of(parts):
        return jnp.concatenate(parts, axis=0).T.astype(BF16)

    for p in range(mix_pieces):
        send_features(0, p)

    for layer in range(layers):
        squares = jnp.zeros((n_tp * rows, 128), F32)
        for p in range(mix_pieces):
            await_bytes(gathered.at[layer, p, pl.ds(0, n_tp - 1)], gather_recv.at[layer, p])
            widened = stack_groups([gathered[layer, p, s].astype(F32) for s in range(n_tp)])
            span = pl.ds(p * piece, piece)
            scaled = (widened * gain[layer, span][None, :]).astype(BF16)
            for lane in range(0, piece, 128):
                tile = widened[:, lane : lane + 128]
                squares = squares + tile * tile
            if p == mix_pieces - 1:
                for c in range(2):
                    sq_part[layer, c] = squares[24 * c : 24 * c + 24]
                remote(
                    sq_part.at[layer, other_core], sq_near.at[layer],
                    send_sem.at[layer, 1], sq_recv.at[layer, 0], "dp", partner,
                )
            for i in range(pieces):
                if p == 0:
                    load_proj(layer, i).wait()
                result = jnp.dot(scaled, proj[layer, i, span, :], preferred_element_type=F32)
                if p > 0:
                    result = result + product[i]
                if p < mix_pieces - 1:
                    product[i] = result
                    continue
                for c in range(2):
                    block = result[24 * c : 24 * c + 24]
                    tail = jnp.concatenate([block[16:, :256], block[16:, 256:]], axis=0)
                    partial[layer, i, c] = jnp.concatenate([block[:16], tail], axis=1).astype(BF16)
                remote(
                    partial.at[layer, i, other_core], near.at[layer, i],
                    send_sem.at[layer, 2], near_recv.at[layer, i], "dp", partner,
                )

        await_bytes(sq_near.at[layer], sq_recv.at[layer, 0])
        chip_squares = sq_part[layer, core] + sq_near[layer]
        sq_cross[layer] = jnp.concatenate(
            [jnp.where(chip == 0, chip_squares[8:16], chip_squares[:8]), chip_squares[16:]], axis=0
        )
        remote(
            sq_cross.at[layer], sq_far.at[layer],
            send_sem.at[layer, 6], sq_recv.at[layer, 1], "dp", across,
        )
        for i in range(pieces):
            await_bytes(near.at[layer, i], near_recv.at[layer, i])
            both = partial[layer, i, core].astype(F32) + near[layer, i].astype(F32)
            tail = jnp.concatenate([both[:8, piece:], both[8:, piece:]], axis=1)
            zero, one = both[:8, :piece], both[8:, :piece]
            cross[layer, i] = fold(jnp.where(chip == 0, one, zero), tail, other_chip).astype(BF16)
            remote(
                cross.at[layer, i], far.at[layer, i],
                send_sem.at[layer, 3], far_recv.at[layer, i], "dp", across,
            )
            own[i] = fold(jnp.where(chip == 0, zero, one), tail, chip)

        await_bytes(sq_far.at[layer], sq_recv.at[layer, 1])
        last = chip_squares[16:] + sq_far[layer, pl.ds(8, 8), :]
        total_squares = jnp.concatenate(
            [
                jnp.where(chip == 0, chip_squares[:8], chip_squares[8:16])
                + sq_far[layer, pl.ds(0, 8), :],
                jnp.where(chip == 0, last, swap(last)),
            ],
            axis=0,
        )
        inverse = lax.rsqrt(jnp.sum(total_squares, axis=1, keepdims=True) / d_model + EPSILON)

        def projected(i):
            await_bytes(far.at[layer, i], far_recv.at[layer, i])
            return unfold_rows(own[i] + far[layer, i].astype(F32)) * inverse

        query = projected(0)
        key = projected(1) * head_key ** (-0.5)
        logits = projected(2)
        log_sigmoid = jnp.minimum(logits, 0.0) - jnp.log(1.0 + jnp.exp(-jnp.abs(logits)))
        log_decay = log_sigmoid[:rows] / SOFTNESS + offset[:, layer, :]
        decay = jnp.exp(jnp.concatenate([log_decay, jnp.zeros((pad - rows, key_cols), F32)], axis=0))
        read_columns = columns_of(split(query * decay))
        both = query * key
        products = [
            jnp.sum(both[:, h * head_key : (h + 1) * head_key], axis=1, keepdims=True)
            for h in range(heads)
        ]
        load_state(layer).wait()
        for pair in range(rows // 2):
            factors = jnp.dot(
                read_columns, expand[0, pair, pl.ds(0, 2 * pad), :], preferred_element_type=F32
            )
            for k in range(2):
                b = 2 * pair + k
                for h in range(heads):
                    factor = factors[
                        h * head_key : (h + 1) * head_key,
                        k * value_channels : (k + 1) * value_channels,
                    ]
                    readout[h, pl.ds(b, 1), :] = jnp.sum(
                        factor * state[layer, b, h], axis=0, keepdims=True
                    )

        for half in range(halves):
            value = projected(3 + 2 * half)
            gate_all = projected(4 + 2 * half)
            values[:, pl.ds(half * piece, piece)] = value
            gated_heads = []
            for hh in range(half_heads):
                h = half * half_heads + hh
                span = slice(hh * value_channels, (hh + 1) * value_channels)
                got = readout[h] + products[h] * value[:, span]
                gate = gate_all[:, span]
                normed = got * lax.rsqrt(jnp.mean(got * got, axis=1, keepdims=True) + EPSILON)
                whole = pl.ds(h * value_channels, value_channels)
                normed = normed * out_gain[layer, whole][None, :]
                gated_heads.append(normed * (gate / (1.0 + jnp.exp(-gate))))
            gated = jnp.concatenate(gated_heads, axis=1)
            gated_all[layer, half, dp] = fold(gated[:8], gated[8:], 0).astype(BF16)
            for j in range(1, n_dp):
                remote(
                    gated_all.at[layer, half, dp], gated_all.at[layer, half, dp],
                    send_sem.at[layer, 4], gated_recv.at[layer, half],
                    "dp", lax.rem(dp + j, n_dp),
                )

        fresh_columns[...] = columns_of(split(key) + split(decay))
        for pair in range(rows // 2):
            adds = jnp.dot(fresh_columns[...], expand[0, pair], preferred_element_type=F32)
            keeps = jnp.dot(fresh_columns[...], expand[1, pair], preferred_element_type=F32)
            for k in range(2):
                b = 2 * pair + k
                lanes = slice(k * value_channels, (k + 1) * value_channels)
                for h in range(heads):
                    part = slice(h * head_key, (h + 1) * head_key)
                    row = values[pl.ds(b, 1), pl.ds(h * value_channels, value_channels)]
                    new_state_ref[layer, b, h] = (
                        keeps[part, lanes] * state[layer, b, h] + adds[part, lanes] * row
                    )

        load_wo(layer).wait()
        for half in range(halves):
            await_bytes(gated_all.at[layer, half, pl.ds(0, n_dp - 1)], gated_recv.at[layer, half])
            gated = stack_groups(
                [gated_all[layer, half, s].astype(F32) for s in range(n_dp)]
            ).astype(BF16)
            for p in range(mix_pieces):
                columns = pl.ds(p * piece, piece)
                result = jnp.dot(
                    gated, wo[layer, pl.ds(half * piece, piece), columns],
                    preferred_element_type=F32,
                )
                if half > 0:
                    result = result + mix_part[p]
                if half < halves - 1:
                    mix_part[p] = result
                    continue
                for s in range(n_tp):
                    mix_send[layer, p, s] = group_of(result, s).astype(BF16)
                for j in range(n_tp - 1, 0, -1):
                    step = tp_step(j)
                    to = lax.rem(tp + step, n_tp)
                    remote(
                        mix_send.at[layer, p, to], mix_recv.at[layer, p, step - 1],
                        send_sem.at[layer, 5], mix_recv_sem.at[layer, p], "tp", to,
                    )

        await_bytes(gathered.at[layer, :, pl.ds(0, n_tp - 1)], send_sem.at[layer, 0])
        await_bytes(sq_near.at[layer], send_sem.at[layer, 1])
        await_bytes(sq_far.at[layer], send_sem.at[layer, 6])
        await_bytes(near.at[layer], send_sem.at[layer, 2])
        await_bytes(far.at[layer], send_sem.at[layer, 3])
        await_bytes(gated_all.at[layer, :, pl.ds(0, n_dp - 1)], send_sem.at[layer, 4])

        for p in range(mix_pieces):
            await_bytes(mix_recv.at[layer, p], mix_recv_sem.at[layer, p])
            total = mix_send[layer, p, tp].astype(F32)
            for j in range(1, n_tp):
                total = total + mix_recv[layer, p, j - 1].astype(F32)
            result = (gathered[layer, p, tp].astype(F32) + total).astype(BF16)
            if layer + 1 < layers:
                gathered[layer + 1, p, tp] = result
                send_features(layer + 1, p)
            else:
                span = slice(p * piece, (p + 1) * piece)
                hidden_out_ref[:, span] = unfold_rows(result.astype(F32))[:rows].astype(BF16)
        await_bytes(mix_recv.at[layer], send_sem.at[layer, 5])


def store_kernel(hidden_ref, state_ref, hidden_out, state_out, hidden_sem, state_sem):
    layers, rows = state_ref.shape[:2]
    copies = [
        pltpu.make_async_copy(state_ref.at[layer, b], state_out.at[layer, b], state_sem.at[layer, b])
        for layer in range(layers)
        for b in range(rows)
    ]
    copies.append(pltpu.make_async_copy(hidden_ref, hidden_out, hidden_sem))
    for copy in copies:
        copy.start()
    for copy in copies:
        copy.wait()


def fused(
    n_tp, n_dp, hidden_in, input_norm_gain, w_query, w_key, w_decay, w_value, w_gate,
    out_gain, w_out, decay_offset, state,
):
    layers, rows, heads, head_key, value_channels = state.shape
    width = hidden_in.shape[1]
    key_cols, value_cols = w_query.shape[2], w_value.shape[2]
    piece = key_cols
    halves = value_cols // piece
    pieces = 3 + 2 * halves
    mix_pieces = width // piece
    block = (16, piece // 4 * 3)
    vmem = pl.BlockSpec(memory_space=pltpu.VMEM)
    hbm = pl.BlockSpec(memory_space=pl.ANY)
    offsets = decay_offset.transpose(1, 0, 2)
    hidden, fresh = pl.pallas_call(
        functools.partial(
            block_kernel, n_tp, n_dp, width * n_dp, head_key, value_channels, piece
        ),
        out_shape=(
            pltpu.VMEM(hidden_in.shape, BF16),
            pltpu.VMEM(state.shape, F32),
        ),
        in_specs=[hbm] * 11,
        out_specs=(vmem, vmem),
        scratch_shapes=[
            pltpu.VMEM(hidden_in.shape, BF16),
            pltpu.VMEM(input_norm_gain.shape, F32),
            pltpu.VMEM(out_gain.shape, F32),
            pltpu.VMEM(offsets.shape, F32),
            pltpu.VMEM((layers, pieces, width, piece), BF16),
            pltpu.VMEM(w_out.shape, BF16),
            pltpu.VMEM(state.shape, F32),
            pltpu.VMEM((layers, mix_pieces, n_tp) + block, BF16),
            pltpu.VMEM((pieces, n_tp * rows, piece), F32),
            pltpu.VMEM((layers, pieces, 2, 16, piece // 2 * 3), BF16),
            pltpu.VMEM((layers, pieces, 16, piece // 2 * 3), BF16),
            pltpu.VMEM((pieces,) + block, F32),
            pltpu.VMEM((layers, pieces) + block, BF16),
            pltpu.VMEM((layers, pieces) + block, BF16),
            pltpu.VMEM((layers, 2, 2 * rows, 128), F32),
            pltpu.VMEM((layers, 2 * rows, 128), F32),
            pltpu.VMEM((layers, 16, 128), F32),
            pltpu.VMEM((layers, 16, 128), F32),
            pltpu.VMEM((2, rows // 2, 64, 2 * value_channels), BF16),
            pltpu.VMEM((16, value_cols), F32),
            pltpu.VMEM((key_cols, 64), BF16),
            pltpu.VMEM((heads, 16, value_channels), F32),
            pltpu.VMEM((layers, halves, n_dp) + block, BF16),
            pltpu.VMEM((mix_pieces, n_tp * rows, piece), F32),
            pltpu.VMEM((layers, mix_pieces, n_tp) + block, BF16),
            pltpu.VMEM((layers, mix_pieces, n_tp - 1) + block, BF16),
            pltpu.SemaphoreType.DMA((4,)),
            pltpu.SemaphoreType.DMA((layers, pieces)),
            pltpu.SemaphoreType.DMA((layers,)),
            pltpu.SemaphoreType.DMA((layers,)),
            pltpu.SemaphoreType.DMA((layers, mix_pieces)),
            pltpu.SemaphoreType.DMA((layers, pieces)),
            pltpu.SemaphoreType.DMA((layers, pieces)),
            pltpu.SemaphoreType.DMA((layers, 2)),
            pltpu.SemaphoreType.DMA((layers, halves)),
            pltpu.SemaphoreType.DMA((layers, mix_pieces)),
            pltpu.SemaphoreType.DMA((layers, 7)),
        ],
        compiler_params=pltpu.CompilerParams(
            collective_id=0, has_side_effects=True, vmem_limit_bytes=48 * 1024 * 1024
        ),
    )(
        hidden_in, input_norm_gain, out_gain, offsets,
        w_query, w_key, w_decay, w_value, w_gate, w_out, state,
    )
    return pl.pallas_call(
        store_kernel,
        out_shape=(
            jax.ShapeDtypeStruct(hidden_in.shape, BF16),
            jax.ShapeDtypeStruct(state.shape, F32),
        ),
        in_specs=[vmem] * 2,
        out_specs=(hbm, hbm),
        scratch_shapes=[
            pltpu.SemaphoreType.DMA,
            pltpu.SemaphoreType.DMA((layers, rows)),
        ],
        compiler_params=pltpu.CompilerParams(vmem_limit_bytes=1024 * 1024),
    )(hidden, fresh)


def plain(
    hidden_in, input_norm_gain, w_query, w_key, w_decay, w_value, w_gate,
    out_gain, w_out, decay_offset, state,
):
    layers, rows, heads, head_key, value_channels = state.shape
    key_cols, value_cols = w_query.shape[2], w_value.shape[2]
    d_model = hidden_in.shape[1] * lax.axis_size("dp")
    first = lax.axis_index("dp") * rows
    current, states = hidden_in, []
    for layer in range(layers):
        widened = lax.all_gather(current, "tp", axis=0, tiled=True).astype(F32)
        squares = lax.psum(jnp.sum(widened * widened, axis=1), "dp")
        scaled = (widened * input_norm_gain[layer][None, :]).astype(BF16)
        partial = jnp.concatenate(
            [
                jnp.dot(scaled, matrix[layer], preferred_element_type=F32)
                for matrix in (w_query, w_key, w_decay, w_value, w_gate)
            ],
            axis=1,
        ).astype(BF16)
        summed = lax.psum_scatter(partial, "dp", scatter_dimension=0, tiled=True).astype(F32)
        own = lax.dynamic_slice_in_dim(squares, first, rows)
        projected = summed * lax.rsqrt(own / d_model + EPSILON)[:, None]
        query, key, logits, value, gate = jnp.split(
            projected,
            [key_cols, 2 * key_cols, 3 * key_cols, 3 * key_cols + value_cols],
            axis=1,
        )
        decay = jnp.exp(jax.nn.log_sigmoid(logits) / SOFTNESS + decay_offset[layer])
        per_key, per_value = (rows, heads, head_key), (rows, heads, value_channels)
        fresh = (
            decay.reshape(per_key)[..., None] * state[layer]
            + (key * head_key ** (-0.5)).reshape(per_key)[..., None]
            * value.reshape(per_value)[:, :, None, :]
        )
        got = jnp.sum(query.reshape(per_key)[..., None] * fresh, axis=2)
        got = got * lax.rsqrt(jnp.mean(got * got, axis=2, keepdims=True) + EPSILON)
        got = got * out_gain[layer].reshape(heads, value_channels)[None]
        gated = (got * jax.nn.silu(gate.reshape(per_value))).reshape(rows, value_cols).astype(BF16)
        mixed = jnp.dot(
            lax.all_gather(gated, "dp", axis=0, tiled=True), w_out[layer],
            preferred_element_type=F32,
        ).astype(BF16)
        mine = lax.psum_scatter(mixed, "tp", scatter_dimension=0, tiled=True).astype(F32)
        current = (current.astype(F32) + mine).astype(BF16)
        states.append(fresh)
    return current, jnp.stack(states)


def solution(mesh):
    n_tp, n_dp = mesh.shape["tp"], mesh.shape["dp"]

    def per_device(hidden_in, *rest):
        state = rest[-1]
        width, key_cols, value_cols = hidden_in.shape[1], rest[1].shape[2], rest[4].shape[2]
        rows, heads = state.shape[1], state.shape[2]
        sized = key_cols == 512 and width % key_cols == 0 and value_cols % key_cols == 0
        shaped = hidden_in.shape[0] == rows == 12 and state.shape[4] == 128
        if n_tp == 4 and n_dp == 4 and sized and shaped and heads % (value_cols // key_cols) == 0:
            return fused(n_tp, n_dp, hidden_in, *rest)
        return plain(hidden_in, *rest)

    return jax.shard_map(
        per_device,
        mesh=mesh,
        in_specs=(
            P(("grp", "tp"), "dp"),
            P(None, "dp"),
            P(None, "dp", "tp"),
            P(None, "dp", "tp"),
            P(None, "dp", "tp"),
            P(None, "dp", "tp"),
            P(None, "dp", "tp"),
            P(None, "tp"),
            P(None, "tp", "dp"),
            P(None, ("grp", "dp"), "tp"),
            P(None, ("grp", "dp"), "tp", None, None),
        ),
        out_specs=(P(("grp", "tp"), "dp"), P(None, ("grp", "dp"), "tp", None, None)),
        check_vma=False,
    )
```

time: 47 us -> 44 us (0.936)
  local copies, waits for them, and re-layouts: 3.32 us -> 0 us
    unnamed x4 -> x0, local copies, waits for them, and re-layouts: 3.32 us -> none
    pallas_call x0 -> x1, Pallas kernels: none -> 2.85 us  [fused(): pl.pallas_call(store_kernel, out_shape=(jax.ShapeDtypeStruct(hidden_in.sh...]
    pallas_call x1, Pallas kernels: 42.8 us -> 40.3 us  [fused(): pl.pallas_call(functools.partial(block_kernel, n_tp, n_dp, width * n_dp,...]
where the time goes in v1:
time: 44 us; the launch traced here: 43.8 us
  Pallas kernels  43.2 us (98%)
  between operations  0.64 us (1%)
    pallas_call x1, Pallas kernels, fused(): pl.pallas_call(functools.partial(block_kernel, n_tp, n_dp, width * n_dp,...  40.3 us
    pallas_call x1, Pallas kernels, fused(): pl.pallas_call(store_kernel, out_shape=(jax.ShapeDtypeStruct(hidden_in.sh...  2.85 us

profile of v1, /device:TPU:0, one launch (start us, length us, event | category | flops | bytes accessed | tf_op | source)
XLA Modules:
  0.0 43.8 jit_solution(16858490097975211951)
XLA Ops:
  0.6 40.3 %shard_map.122 = (bf16[12,1024]{1,0:T(8,128)(2,1)S(1)}, f32[2,12,8,64,128]{4,3,2,1,0:T(8,128)S(1)}) custom-call(bf16[12,1024]{1,0:T(8,128)(2,1)} %hidden_hbm.1, f32[2,1024]{1,0:T(2,128)} %gain_hbm.1, f32[2,1024]{1,0:T(2,128)} %out_gain_hbm.1, f32[12,2,512]{2,1,0:T(2,128)} %bitcast.1, bf16[2,1024,512]{2,1,0:T(8,128)(2,1)} %wq_hbm.1, ...), custom_call_target="tpu_custom_call" | custom-call | tf_op jit(solution)/shard_map/pallas_call | solution.py:414
  41.0 2.9 %shard_map.123 = (bf16[12,1024]{1,0:T(8,128)(2,1)}, f32[2,12,8,64,128]{4,3,2,1,0:T(8,128)}) custom-call(bf16[12,1024]{1,0:T(8,128)(2,1)S(1)} %get-tuple-element.4.hidden_ref, f32[2,12,8,64,128]{4,3,2,1,0:T(8,128)S(1)} %get-tuple-element.5.state_ref), custom_call_target="tpu_custom_call" | custom-call | tf_op jit(solution)/shard_map/pallas_call | solution.py:470

commit v2 on v1

--- a/solution.py
+++ b/solution.py
@@ -83,7 +83,7 @@
     gathered, product, partial, near, own, cross, far,
     sq_part, sq_near, sq_cross, sq_far,
     expand, values, fresh_columns, readout,
-    gated_all, mix_part, mix_send, mix_recv,
+    gated_all, mix_part, mix_send, mix_recv, mix_last,
     small_sem, proj_sem, wo_sem, state_sem,
     gather_recv, near_recv, far_recv, sq_recv, gated_recv, mix_recv_sem, send_sem,
 ):
@@ -95,6 +95,8 @@
     value_cols = heads * value_channels
     halves = value_cols // piece
     half_heads = heads // halves
+    groups = ((0, 3), (3, pieces - 3))
+    parcels = ((0, 1), (1, 1), (2, 1)) + tuple((3 + 2 * half, 2) for half in range(halves))
     tp = lax.axis_index("tp")
     dp = lax.axis_index("dp")
     chip, core = dp // 2, lax.rem(dp, 2)
@@ -123,17 +125,17 @@
 
     def load_proj(layer, i):
         if i < 3:
-            source = (wq_hbm, wk_hbm, wd_hbm)[i].at[layer]
+            source = (wd_hbm, wq_hbm, wk_hbm)[i].at[layer]
         else:
             half, which = divmod(i - 3, 2)
             source = (wv_hbm, wg_hbm)[which].at[layer, :, pl.ds(half * piece, piece)]
-        return pltpu.make_async_copy(source, proj.at[layer, i], proj_sem.at[layer, i])
+        return pltpu.make_async_copy(source, proj.at[layer, i], proj_sem.at[layer])
 
     def load_wo(layer):
-        return pltpu.make_async_copy(wo_hbm.at[layer], wo.at[layer], wo_sem.at[layer])
+        return pltpu.make_async_copy(wo_hbm.at[layer], wo.at[layer], wo_sem)
 
     def load_state(layer):
-        return pltpu.make_async_copy(state_hbm.at[layer], state.at[layer], state_sem.at[layer])
+        return pltpu.make_async_copy(state_hbm.at[layer], state.at[layer], state_sem)
 
     for copy in small:
         copy.start()
@@ -173,7 +175,8 @@
     def await_bytes(ref, sem):
         pltpu.make_async_copy(ref, ref, sem).wait()
 
-    above = tp // (n_tp // 2)
+    above = tp // 2
+    is_owner = (tp == 1) | (tp == 2)
 
     def tp_step(j):
         return j + above * (n_tp - 2 * j)
@@ -182,9 +185,88 @@
         for j in range(n_tp - 1, 0, -1):
             remote(
                 gathered.at[layer, p, tp], gathered.at[layer, p, tp],
-                send_sem.at[layer, 0], gather_recv.at[layer, p],
+                send_sem.at[0], gather_recv.at[p],
                 "tp", lax.rem(tp + tp_step(j), n_tp),
             )
+
+    def await_features(layer, p):
+        if layer == 0:
+            await_bytes(gathered.at[layer, p, pl.ds(0, n_tp - 1)], gather_recv.at[p])
+            return
+
+        @pl.when(is_owner)
+        def _():
+            await_bytes(gathered.at[layer, p, pl.ds(0, 2)], gather_recv.at[p])
+
+        @pl.when(jnp.logical_not(is_owner))
+        def _():
+            await_bytes(gathered.at[layer, p], gather_recv.at[p])
+
+    def await_feature_sends(layer):
+        if layer == 0:
+            await_bytes(gathered.at[layer, :, pl.ds(0, n_tp - 1)], send_sem.at[0])
+            return
+
+        @pl.when(is_owner)
+        def _():
+            await_bytes(mix_recv.at[layer - 1], send_sem.at[0])
+
+    def send_mixed(layer, p):
+        for k in range(2):
+
+            def send_to(owner):
+                remote(
+                    mix_send.at[layer, p, 2 * (owner - 1) + k],
+                    mix_recv.at[layer, p, k, tp - above],
+                    send_sem.at[5], mix_recv_sem.at[p, k], "tp", owner,
+                )
+
+            send_to(2 - above)
+
+            @pl.when(jnp.logical_not(is_owner))
+            def _():
+                send_to(1 + above)
+
+    lowest = tp == 0
+    last_order = (
+        jnp.where(lowest, 3, 0),
+        jnp.where(lowest, 2, 1 + lax.rem(tp, 3)),
+        jnp.where(lowest, 1, 1 + lax.rem(tp + 1, 3)),
+    )
+
+    def send_last(layer, p, to):
+        remote(
+            mix_send.at[layer, p, to], mix_last.at[p, lax.rem(tp - to + n_tp - 1, n_tp)],
+            send_sem.at[5], mix_recv_sem.at[p, 0], "tp", to,
+        )
+
+    def await_mixed_sends(layer):
+        if layer == layers - 1:
+            await_bytes(mix_last, send_sem.at[5])
+            return
+
+        @pl.when(is_owner)
+        def _():
+            await_bytes(mix_send.at[layer, :, pl.ds(0, 2)], send_sem.at[5])
+
+        @pl.when(jnp.logical_not(is_owner))
+        def _():
+            await_bytes(mix_send.at[layer], send_sem.at[5])
+
+    def finish_middle(layer):
+        for p in range(mix_pieces):
+            for k in range(2):
+                await_bytes(mix_recv.at[layer, p, k], mix_recv_sem.at[p, k])
+                mine = 2 * (tp - 1) + k
+                total = mix_send[layer, p, mine].astype(F32)
+                for j in range(n_tp - 1):
+                    total = total + mix_recv[layer, p, k, j].astype(F32)
+                gathered[layer + 1, p, mine] = (
+                    gathered[layer, p, mine].astype(F32) + total
+                ).astype(BF16)
+                block = gathered.at[layer + 1, p, mine]
+                for to in (3 * (2 - tp), 3 - tp, 3 * (tp - 1)):
+                    remote(block, block, send_sem.at[0], gather_recv.at[p], "tp", to)
 
     def split(block):
         high = block.astype(BF16).astype(F32)
@@ -199,7 +281,7 @@
     for layer in range(layers):
         squares = jnp.zeros((n_tp * rows, 128), F32)
         for p in range(mix_pieces):
-            await_bytes(gathered.at[layer, p, pl.ds(0, n_tp - 1)], gather_recv.at[layer, p])
+            await_features(layer, p)
             widened = stack_groups([gathered[layer, p, s].astype(F32) for s in range(n_tp)])
             span = pl.ds(p * piece, piece)
             scaled = (widened * gain[layer, span][None, :]).astype(BF16)
@@ -211,48 +293,58 @@
                     sq_part[layer, c] = squares[24 * c : 24 * c + 24]
                 remote(
                     sq_part.at[layer, other_core], sq_near.at[layer],
-                    send_sem.at[layer, 1], sq_recv.at[layer, 0], "dp", partner,
+                    send_sem.at[1], sq_recv.at[0], "dp", partner,
                 )
-            for i in range(pieces):
-                if p == 0:
-                    load_proj(layer, i).wait()
-                result = jnp.dot(scaled, proj[layer, i, span, :], preferred_element_type=F32)
-                if p > 0:
-                    result = result + product[i]
-                if p < mix_pieces - 1:
-                    product[i] = result
-                    continue
-                for c in range(2):
-                    block = result[24 * c : 24 * c + 24]
-                    tail = jnp.concatenate([block[16:, :256], block[16:, 256:]], axis=0)
-                    partial[layer, i, c] = jnp.concatenate([block[:16], tail], axis=1).astype(BF16)
-                remote(
-                    partial.at[layer, i, other_core], near.at[layer, i],
-                    send_sem.at[layer, 2], near_recv.at[layer, i], "dp", partner,
-                )
-
-        await_bytes(sq_near.at[layer], sq_recv.at[layer, 0])
+            if p == 0:
+                await_bytes(proj.at[layer], proj_sem.at[layer])
+            for first, count in groups:
+                for i in range(first, first + count):
+                    result = jnp.dot(scaled, proj[layer, i, span, :], preferred_element_type=F32)
+                    if p > 0:
+                        result = result + product[i]
+                    if p < mix_pieces - 1:
+                        product[i] = result
+                        continue
+                    for c in range(2):
+                        block = result[24 * c : 24 * c + 24]
+                        tail = jnp.concatenate([block[16:, :256], block[16:, 256:]], axis=0)
+                        partial[layer, c, i] = jnp.concatenate(
+                            [block[:16], tail], axis=1
+                        ).astype(BF16)
+                if p == mix_pieces - 1:
+                    these = pl.ds(first, count)
+                    remote(
+                        partial.at[layer, other_core, these], near.at[layer, these],
+                        send_sem.at[2], near_recv.at[min(first, 1)], "dp", partner,
+                    )
+
+        await_bytes(sq_near.at[layer], sq_recv.at[0])
         chip_squares = sq_part[layer, core] + sq_near[layer]
         sq_cross[layer] = jnp.concatenate(
             [jnp.where(chip == 0, chip_squares[8:16], chip_squares[:8]), chip_squares[16:]], axis=0
         )
         remote(
             sq_cross.at[layer], sq_far.at[layer],
-            send_sem.at[layer, 6], sq_recv.at[layer, 1], "dp", across,
+            send_sem.at[6], sq_recv.at[1], "dp", across,
         )
         for i in range(pieces):
-            await_bytes(near.at[layer, i], near_recv.at[layer, i])
-            both = partial[layer, i, core].astype(F32) + near[layer, i].astype(F32)
+            for first, count in groups:
+                if i == first:
+                    await_bytes(near.at[layer, pl.ds(first, count)], near_recv.at[min(first, 1)])
+            both = partial[layer, core, i].astype(F32) + near[layer, i].astype(F32)
             tail = jnp.concatenate([both[:8, piece:], both[8:, piece:]], axis=1)
             zero, one = both[:8, :piece], both[8:, :piece]
             cross[layer, i] = fold(jnp.where(chip == 0, one, zero), tail, other_chip).astype(BF16)
-            remote(
-                cross.at[layer, i], far.at[layer, i],
-                send_sem.at[layer, 3], far_recv.at[layer, i], "dp", across,
-            )
+            for number, (first, count) in enumerate(parcels):
+                if i == first + count - 1:
+                    these = pl.ds(first, count)
+                    remote(
+                        cross.at[layer, these], far.at[layer, these],
+                        send_sem.at[3], far_recv.at[number], "dp", across,
+                    )
             own[i] = fold(jnp.where(chip == 0, zero, one), tail, chip)
 
-        await_bytes(sq_far.at[layer], sq_recv.at[layer, 1])
+        await_bytes(sq_far.at[layer], sq_recv.at[1])
         last = chip_squares[16:] + sq_far[layer, pl.ds(8, 8), :]
         total_squares = jnp.concatenate(
             [
@@ -265,44 +357,49 @@
         inverse = lax.rsqrt(jnp.sum(total_squares, axis=1, keepdims=True) / d_model + EPSILON)
 
         def projected(i):
-            await_bytes(far.at[layer, i], far_recv.at[layer, i])
+            for number, (first, count) in enumerate(parcels):
+                if i == first:
+                    await_bytes(far.at[layer, pl.ds(first, count)], far_recv.at[number])
             return unfold_rows(own[i] + far[layer, i].astype(F32)) * inverse
 
-        query = projected(0)
-        key = projected(1) * head_key ** (-0.5)
-        logits = projected(2)
+        if layer == 0:
+            await_bytes(state, state_sem)
+        logits = projected(0)
         log_sigmoid = jnp.minimum(logits, 0.0) - jnp.log(1.0 + jnp.exp(-jnp.abs(logits)))
         log_decay = log_sigmoid[:rows] / SOFTNESS + offset[:, layer, :]
         decay = jnp.exp(jnp.concatenate([log_decay, jnp.zeros((pad - rows, key_cols), F32)], axis=0))
+        query = projected(1)
         read_columns = columns_of(split(query * decay))
+        key = projected(2) * head_key ** (-0.5)
         both = query * key
         products = [
             jnp.sum(both[:, h * head_key : (h + 1) * head_key], axis=1, keepdims=True)
             for h in range(heads)
         ]
-        load_state(layer).wait()
-        for pair in range(rows // 2):
-            factors = jnp.dot(
-                read_columns, expand[0, pair, pl.ds(0, 2 * pad), :], preferred_element_type=F32
-            )
-            for k in range(2):
-                b = 2 * pair + k
-                for h in range(heads):
-                    factor = factors[
-                        h * head_key : (h + 1) * head_key,
-                        k * value_channels : (k + 1) * value_channels,
-                    ]
-                    readout[h, pl.ds(b, 1), :] = jnp.sum(
-                        factor * state[layer, b, h], axis=0, keepdims=True
-                    )
 
         for half in range(halves):
+            base = half * half_heads
+            columns = read_columns[base * head_key : (base + half_heads) * head_key]
+            for pair in range(rows // 2):
+                factors = jnp.dot(
+                    columns, expand[0, pair, pl.ds(0, 2 * pad), :], preferred_element_type=F32
+                )
+                for k in range(2):
+                    b = 2 * pair + k
+                    for hh in range(half_heads):
+                        factor = factors[
+                            hh * head_key : (hh + 1) * head_key,
+                            k * value_channels : (k + 1) * value_channels,
+                        ]
+                        readout[base + hh, pl.ds(b, 1), :] = jnp.sum(
+                            factor * state[layer, b, base + hh], axis=0, keepdims=True
+                        )
             value = projected(3 + 2 * half)
             gate_all = projected(4 + 2 * half)
             values[:, pl.ds(half * piece, piece)] = value
             gated_heads = []
             for hh in range(half_heads):
-                h = half * half_heads + hh
+                h = base + hh
                 span = slice(hh * value_channels, (hh + 1) * value_channels)
                 got = readout[h] + products[h] * value[:, span]
                 gate = gate_all[:, span]
@@ -315,7 +412,7 @@
             for j in range(1, n_dp):
                 remote(
                     gated_all.at[layer, half, dp], gated_all.at[layer, half, dp],
-                    send_sem.at[layer, 4], gated_recv.at[layer, half],
+                    send_sem.at[4], gated_recv.at[half],
                     "dp", lax.rem(dp + j, n_dp),
                 )
 
@@ -333,9 +430,10 @@
                         keeps[part, lanes] * state[layer, b, h] + adds[part, lanes] * row
                     )
 
-        load_wo(layer).wait()
+        if layer == 0:
+            await_bytes(wo, wo_sem)
         for half in range(halves):
-            await_bytes(gated_all.at[layer, half, pl.ds(0, n_dp - 1)], gated_recv.at[layer, half])
+            await_bytes(gated_all.at[layer, half, pl.ds(0, n_dp - 1)], gated_recv.at[half])
             gated = stack_groups(
                 [gated_all[layer, half, s].astype(F32) for s in range(n_dp)]
             ).astype(BF16)
@@ -352,48 +450,48 @@
                     continue
                 for s in range(n_tp):
                     mix_send[layer, p, s] = group_of(result, s).astype(BF16)
-                for j in range(n_tp - 1, 0, -1):
-                    step = tp_step(j)
-                    to = lax.rem(tp + step, n_tp)
-                    remote(
-                        mix_send.at[layer, p, to], mix_recv.at[layer, p, step - 1],
-                        send_sem.at[layer, 5], mix_recv_sem.at[layer, p], "tp", to,
-                    )
-
-        await_bytes(gathered.at[layer, :, pl.ds(0, n_tp - 1)], send_sem.at[layer, 0])
-        await_bytes(sq_near.at[layer], send_sem.at[layer, 1])
-        await_bytes(sq_far.at[layer], send_sem.at[layer, 6])
-        await_bytes(near.at[layer], send_sem.at[layer, 2])
-        await_bytes(far.at[layer], send_sem.at[layer, 3])
-        await_bytes(gated_all.at[layer, :, pl.ds(0, n_dp - 1)], send_sem.at[layer, 4])
-
-        for p in range(mix_pieces):
-            await_bytes(mix_recv.at[layer, p], mix_recv_sem.at[layer, p])
-            total = mix_send[layer, p, tp].astype(F32)
-            for j in range(1, n_tp):
-                total = total + mix_recv[layer, p, j - 1].astype(F32)
-            result = (gathered[layer, p, tp].astype(F32) + total).astype(BF16)
-            if layer + 1 < layers:
-                gathered[layer + 1, p, tp] = result
-                send_features(layer + 1, p)
-            else:
+                if layer < layers - 1:
+                    send_mixed(layer, p)
+                else:
+                    send_last(layer, p, last_order[0])
+
+        if layer == layers - 1:
+            for to in last_order[1:]:
+                for p in range(mix_pieces):
+                    send_last(layer, p, to)
+
+        await_feature_sends(layer)
+        await_bytes(sq_near.at[layer], send_sem.at[1])
+        await_bytes(sq_far.at[layer], send_sem.at[6])
+        await_bytes(near.at[layer], send_sem.at[2])
+        await_bytes(far.at[layer], send_sem.at[3])
+        await_bytes(gated_all.at[layer, :, pl.ds(0, n_dp - 1)], send_sem.at[4])
+
+        if layer + 1 < layers:
+            pl.when(is_owner)(functools.partial(finish_middle, layer))
+        else:
+            for p in range(mix_pieces):
+                await_bytes(mix_last.at[p], mix_recv_sem.at[p, 0])
+                total = mix_send[layer, p, tp].astype(F32)
+                for j in range(n_tp - 1):
+                    total = total + mix_last[p, j].astype(F32)
+                result = (gathered[layer, p, tp].astype(F32) + total).astype(BF16)
                 span = slice(p * piece, (p + 1) * piece)
                 hidden_out_ref[:, span] = unfold_rows(result.astype(F32))[:rows].astype(BF16)
-        await_bytes(mix_recv.at[layer], send_sem.at[layer, 5])
+        await_mixed_sends(layer)
 
 
 def store_kernel(hidden_ref, state_ref, hidden_out, state_out, hidden_sem, state_sem):
-    layers, rows = state_ref.shape[:2]
-    copies = [
-        pltpu.make_async_copy(state_ref.at[layer, b], state_out.at[layer, b], state_sem.at[layer, b])
-        for layer in range(layers)
-        for b in range(rows)
-    ]
-    copies.append(pltpu.make_async_copy(hidden_ref, hidden_out, hidden_sem))
-    for copy in copies:
-        copy.start()
-    for copy in copies:
-        copy.wait()
+    layers, rows, heads = state_ref.shape[:3]
+    for layer in range(layers):
+        for b in range(rows):
+            for half in range(2):
+                part = (layer, b, pl.ds(half * (heads // 2), heads // 2))
+                pltpu.make_async_copy(state_ref.at[part], state_out.at[part], state_sem).start()
+    store_hidden = pltpu.make_async_copy(hidden_ref, hidden_out, hidden_sem)
+    store_hidden.start()
+    store_hidden.wait()
+    pltpu.make_async_copy(state_ref, state_out, state_sem).wait()
 
 
 def fused(
@@ -431,7 +529,7 @@
             pltpu.VMEM(state.shape, F32),
             pltpu.VMEM((layers, mix_pieces, n_tp) + block, BF16),
             pltpu.VMEM((pieces, n_tp * rows, piece), F32),
-            pltpu.VMEM((layers, pieces, 2, 16, piece // 2 * 3), BF16),
+            pltpu.VMEM((layers, 2, pieces, 16, piece // 2 * 3), BF16),
             pltpu.VMEM((layers, pieces, 16, piece // 2 * 3), BF16),
             pltpu.VMEM((pieces,) + block, F32),
             pltpu.VMEM((layers, pieces) + block, BF16),
@@ -447,18 +545,19 @@
             pltpu.VMEM((layers, halves, n_dp) + block, BF16),
             pltpu.VMEM((mix_pieces, n_tp * rows, piece), F32),
             pltpu.VMEM((layers, mix_pieces, n_tp) + block, BF16),
-            pltpu.VMEM((layers, mix_pieces, n_tp - 1) + block, BF16),
+            pltpu.VMEM((layers - 1, mix_pieces, 2, n_tp - 1) + block, BF16),
+            pltpu.VMEM((mix_pieces, n_tp - 1) + block, BF16),
             pltpu.SemaphoreType.DMA((4,)),
-            pltpu.SemaphoreType.DMA((layers, pieces)),
             pltpu.SemaphoreType.DMA((layers,)),
-            pltpu.SemaphoreType.DMA((layers,)),
-            pltpu.SemaphoreType.DMA((layers, mix_pieces)),
-            pltpu.SemaphoreType.DMA((layers, pieces)),
-            pltpu.SemaphoreType.DMA((layers, pieces)),
-            pltpu.SemaphoreType.DMA((layers, 2)),
-            pltpu.SemaphoreType.DMA((layers, halves)),
-            pltpu.SemaphoreType.DMA((layers, mix_pieces)),
-            pltpu.SemaphoreType.DMA((layers, 7)),
+            pltpu.SemaphoreType.DMA,
+            pltpu.SemaphoreType.DMA,
+            pltpu.SemaphoreType.DMA((mix_pieces,)),
+            pltpu.SemaphoreType.DMA((2,)),
+            pltpu.SemaphoreType.DMA((3 + halves,)),
+            pltpu.SemaphoreType.DMA((2,)),
+            pltpu.SemaphoreType.DMA((halves,)),
+            pltpu.SemaphoreType.DMA((mix_pieces, 2)),
+            pltpu.SemaphoreType.DMA((7,)),
         ],
         compiler_params=pltpu.CompilerParams(
             collective_id=0, has_side_effects=True, vmem_limit_bytes=48 * 1024 * 1024
@@ -477,7 +576,7 @@
         out_specs=(hbm, hbm),
         scratch_shapes=[
             pltpu.SemaphoreType.DMA,
-            pltpu.SemaphoreType.DMA((layers, rows)),
+            pltpu.SemaphoreType.DMA,
         ],
         compiler_params=pltpu.CompilerParams(vmem_limit_bytes=1024 * 1024),
     )(hidden, fresh)
@@ -538,10 +637,10 @@
     def per_device(hidden_in, *rest):
         state = rest[-1]
         width, key_cols, value_cols = hidden_in.shape[1], rest[1].shape[2], rest[4].shape[2]
-        rows, heads = state.shape[1], state.shape[2]
+        layers, rows, heads = state.shape[:3]
         sized = key_cols == 512 and width % key_cols == 0 and value_cols % key_cols == 0
         shaped = hidden_in.shape[0] == rows == 12 and state.shape[4] == 128
-        if n_tp == 4 and n_dp == 4 and sized and shaped and heads % (value_cols // key_cols) == 0:
+        if n_tp == 4 and n_dp == 4 and layers > 1 and sized and shaped and heads % (value_cols // key_cols) == 0:
             return fused(n_tp, n_dp, hidden_in, *rest)
         return plain(hidden_in, *rest)
 

time: 44 us -> 41.3 us (0.939)
  Pallas kernels: 43.2 us -> 40.5 us
    pallas_call x1, Pallas kernels: 40.3 us -> 37.9 us  [fused(): pl.pallas_call(functools.partial(block_kernel, n_tp, n_dp, width * n_dp,...]
where the time goes in v2:
time: 41.3 us; the launch traced here: 41.1 us
  Pallas kernels  40.5 us (98%)
  between operations  0.64 us (2%)
    pallas_call x1, Pallas kernels, fused(): pl.pallas_call(functools.partial(block_kernel, n_tp, n_dp, width * n_dp,...  37.9 us
    pallas_call x1, Pallas kernels, fused(): pl.pallas_call(store_kernel, out_shape=(jax.ShapeDtypeStruct(hidden_in.sh...  2.62 us

profile of v2, /device:TPU:0, one launch (start us, length us, event | category | flops | bytes accessed | tf_op | source)
XLA Modules:
  0.0 41.1 jit_solution(1486717399911054758)
XLA Ops:
  0.6 37.9 %shard_map.122 = (bf16[12,1024]{1,0:T(8,128)(2,1)S(1)}, f32[2,12,8,64,128]{4,3,2,1,0:T(8,128)S(1)}) custom-call(bf16[12,1024]{1,0:T(8,128)(2,1)} %hidden_hbm.1, f32[2,1024]{1,0:T(2,128)} %gain_hbm.1, f32[2,1024]{1,0:T(2,128)} %out_gain_hbm.1, f32[12,2,512]{2,1,0:T(2,128)} %bitcast.1, bf16[2,1024,512]{2,1,0:T(8,128)(2,1)} %wq_hbm.1, ...), custom_call_target="tpu_custom_call" | custom-call | tf_op jit(solution)/shard_map/pallas_call | solution.py:512
  38.5 2.6 %shard_map.123 = (bf16[12,1024]{1,0:T(8,128)(2,1)}, f32[2,12,8,64,128]{4,3,2,1,0:T(8,128)}) custom-call(bf16[12,1024]{1,0:T(8,128)(2,1)S(1)} %get-tuple-element.4.hidden_ref, f32[2,12,8,64,128]{4,3,2,1,0:T(8,128)S(1)} %get-tuple-element.5.state_ref), custom_call_target="tpu_custom_call" | custom-call | tf_op jit(solution)/shard_map/pallas_call | solution.py:569

commit v3 on v2

--- a/solution.py
+++ b/solution.py
@@ -95,8 +95,9 @@
     value_cols = heads * value_channels
     halves = value_cols // piece
     half_heads = heads // halves
-    groups = ((0, 3), (3, pieces - 3))
-    parcels = ((0, 1), (1, 1), (2, 1)) + tuple((3 + 2 * half, 2) for half in range(halves))
+    pairs = tuple((3 + 2 * half, 2) for half in range(halves))
+    groups = ((0, 3),) + pairs
+    parcels = ((0, 1), (1, 1), (2, 1)) + pairs
     tp = lax.axis_index("tp")
     dp = lax.axis_index("dp")
     chip, core = dp // 2, lax.rem(dp, 2)
@@ -268,6 +269,48 @@
                 for to in (3 * (2 - tp), 3 - tp, 3 * (tp - 1)):
                     remote(block, block, send_sem.at[0], gather_recv.at[p], "tp", to)
 
+    def store_partial(layer, i, result):
+        for c in range(2):
+            block = result[24 * c : 24 * c + 24]
+            tail = jnp.concatenate([block[16:, :256], block[16:, 256:]], axis=0)
+            partial[layer, c, i] = jnp.concatenate([block[:16], tail], axis=1).astype(BF16)
+
+    def send_group(layer, number):
+        these = pl.ds(*groups[number])
+        remote(
+            partial.at[layer, other_core, these], near.at[layer, these],
+            send_sem.at[2], near_recv.at[number], "dp", partner,
+        )
+
+    def cross_first(layer):
+        await_bytes(sq_near.at[layer], sq_recv.at[0])
+        chip_squares = sq_part[layer, core] + sq_near[layer]
+        sq_part[layer, core] = chip_squares
+        sq_cross[layer] = jnp.concatenate(
+            [jnp.where(chip == 0, chip_squares[8:16], chip_squares[:8]), chip_squares[16:]], axis=0
+        )
+        remote(
+            sq_cross.at[layer], sq_far.at[layer], send_sem.at[6], sq_recv.at[1], "dp", across
+        )
+        cross_group(layer, 0)
+
+    def cross_group(layer, number):
+        begin, amount = groups[number]
+        await_bytes(near.at[layer, pl.ds(begin, amount)], near_recv.at[number])
+        for i in range(begin, begin + amount):
+            both = partial[layer, core, i].astype(F32) + near[layer, i].astype(F32)
+            tail = jnp.concatenate([both[:8, piece:], both[8:, piece:]], axis=1)
+            zero, one = both[:8, :piece], both[8:, :piece]
+            cross[layer, i] = fold(jnp.where(chip == 0, one, zero), tail, other_chip).astype(BF16)
+            for parcel, (first, count) in enumerate(parcels):
+                if i == first + count - 1:
+                    these = pl.ds(first, count)
+                    remote(
+                        cross.at[layer, these], far.at[layer, these],
+                        send_sem.at[3], far_recv.at[parcel], "dp", across,
+                    )
+            own[i] = fold(jnp.where(chip == 0, zero, one), tail, chip)
+
     def split(block):
         high = block.astype(BF16).astype(F32)
         return [high, block - high]
@@ -280,14 +323,18 @@
 
     for layer in range(layers):
         squares = jnp.zeros((n_tp * rows, 128), F32)
+        scaled = []
+        first, count = groups[0]
         for p in range(mix_pieces):
             await_features(layer, p)
             widened = stack_groups([gathered[layer, p, s].astype(F32) for s in range(n_tp)])
             span = pl.ds(p * piece, piece)
-            scaled = (widened * gain[layer, span][None, :]).astype(BF16)
+            scaled.append((widened * gain[layer, span][None, :]).astype(BF16))
             for lane in range(0, piece, 128):
                 tile = widened[:, lane : lane + 128]
                 squares = squares + tile * tile
+            if p == 0:
+                await_bytes(proj.at[layer], proj_sem.at[layer])
             if p == mix_pieces - 1:
                 for c in range(2):
                     sq_part[layer, c] = squares[24 * c : 24 * c + 24]
@@ -295,56 +342,30 @@
                     sq_part.at[layer, other_core], sq_near.at[layer],
                     send_sem.at[1], sq_recv.at[0], "dp", partner,
                 )
-            if p == 0:
-                await_bytes(proj.at[layer], proj_sem.at[layer])
-            for first, count in groups:
-                for i in range(first, first + count):
-                    result = jnp.dot(scaled, proj[layer, i, span, :], preferred_element_type=F32)
-                    if p > 0:
-                        result = result + product[i]
-                    if p < mix_pieces - 1:
-                        product[i] = result
-                        continue
-                    for c in range(2):
-                        block = result[24 * c : 24 * c + 24]
-                        tail = jnp.concatenate([block[16:, :256], block[16:, 256:]], axis=0)
-                        partial[layer, c, i] = jnp.concatenate(
-                            [block[:16], tail], axis=1
-                        ).astype(BF16)
-                if p == mix_pieces - 1:
-                    these = pl.ds(first, count)
-                    remote(
-                        partial.at[layer, other_core, these], near.at[layer, these],
-                        send_sem.at[2], near_recv.at[min(first, 1)], "dp", partner,
-                    )
-
-        await_bytes(sq_near.at[layer], sq_recv.at[0])
-        chip_squares = sq_part[layer, core] + sq_near[layer]
-        sq_cross[layer] = jnp.concatenate(
-            [jnp.where(chip == 0, chip_squares[8:16], chip_squares[:8]), chip_squares[16:]], axis=0
-        )
-        remote(
-            sq_cross.at[layer], sq_far.at[layer],
-            send_sem.at[6], sq_recv.at[1], "dp", across,
-        )
-        for i in range(pieces):
-            for first, count in groups:
-                if i == first:
-                    await_bytes(near.at[layer, pl.ds(first, count)], near_recv.at[min(first, 1)])
-            both = partial[layer, core, i].astype(F32) + near[layer, i].astype(F32)
-            tail = jnp.concatenate([both[:8, piece:], both[8:, piece:]], axis=1)
-            zero, one = both[:8, :piece], both[8:, :piece]
-            cross[layer, i] = fold(jnp.where(chip == 0, one, zero), tail, other_chip).astype(BF16)
-            for number, (first, count) in enumerate(parcels):
-                if i == first + count - 1:
-                    these = pl.ds(first, count)
-                    remote(
-                        cross.at[layer, these], far.at[layer, these],
-                        send_sem.at[3], far_recv.at[number], "dp", across,
-                    )
-            own[i] = fold(jnp.where(chip == 0, zero, one), tail, chip)
+            for i in range(first, first + count):
+                result = jnp.dot(scaled[p], proj[layer, i, span, :], preferred_element_type=F32)
+                if p > 0:
+                    result = result + product[i]
+                if p < mix_pieces - 1:
+                    product[i] = result
+                else:
+                    store_partial(layer, i, result)
+        send_group(layer, 0)
+        pl.when(core == 0)(functools.partial(cross_first, layer))
+        whole_rows = jnp.concatenate(scaled, axis=1)
+        for number in range(1, len(groups)):
+            first, count = groups[number]
+            for i in range(first, first + count):
+                store_partial(
+                    layer, i, jnp.dot(whole_rows, proj[layer, i], preferred_element_type=F32)
+                )
+            send_group(layer, number)
+        pl.when(core != 0)(functools.partial(cross_first, layer))
+        for number in range(1, len(groups)):
+            cross_group(layer, number)
 
         await_bytes(sq_far.at[layer], sq_recv.at[1])
+        chip_squares = sq_part[layer, core]
         last = chip_squares[16:] + sq_far[layer, pl.ds(8, 8), :]
         total_squares = jnp.concatenate(
             [
@@ -528,7 +549,7 @@
             pltpu.VMEM(w_out.shape, BF16),
             pltpu.VMEM(state.shape, F32),
             pltpu.VMEM((layers, mix_pieces, n_tp) + block, BF16),
-            pltpu.VMEM((pieces, n_tp * rows, piece), F32),
+            pltpu.VMEM((3, n_tp * rows, piece), F32),
             pltpu.VMEM((layers, 2, pieces, 16, piece // 2 * 3), BF16),
             pltpu.VMEM((layers, pieces, 16, piece // 2 * 3), BF16),
             pltpu.VMEM((pieces,) + block, F32),
@@ -552,7 +573,7 @@
             pltpu.SemaphoreType.DMA,
             pltpu.SemaphoreType.DMA,
             pltpu.SemaphoreType.DMA((mix_pieces,)),
-            pltpu.SemaphoreType.DMA((2,)),
+            pltpu.SemaphoreType.DMA((1 + halves,)),
             pltpu.SemaphoreType.DMA((3 + halves,)),
             pltpu.SemaphoreType.DMA((2,)),
             pltpu.SemaphoreType.DMA((halves,)),

time: 41.3 us -> 40.2 us (0.973)
  Pallas kernels: 40.5 us -> 39.4 us
    pallas_call x1, Pallas kernels: 37.9 us -> 36.8 us  [fused(): pl.pallas_call(functools.partial(block_kernel, n_tp, n_dp, width * n_dp,...]
where the time goes in v3:
time: 40.2 us; the launch traced here: 40.1 us
  Pallas kernels  39.4 us (98%)
  between operations  0.64 us (2%)
    pallas_call x1, Pallas kernels, fused(): pl.pallas_call(functools.partial(block_kernel, n_tp, n_dp, width * n_dp,...  36.8 us
    pallas_call x1, Pallas kernels, fused(): pl.pallas_call(store_kernel, out_shape=(jax.ShapeDtypeStruct(hidden_in.sh...  2.62 us

profile of v3, /device:TPU:0, one launch (start us, length us, event | category | flops | bytes accessed | tf_op | source)
XLA Modules:
  0.0 40.1 jit_solution(15276283299612360468)
XLA Ops:
  0.6 36.8 %shard_map.122 = (bf16[12,1024]{1,0:T(8,128)(2,1)S(1)}, f32[2,12,8,64,128]{4,3,2,1,0:T(8,128)S(1)}) custom-call(bf16[12,1024]{1,0:T(8,128)(2,1)} %hidden_hbm.1, f32[2,1024]{1,0:T(2,128)} %gain_hbm.1, f32[2,1024]{1,0:T(2,128)} %out_gain_hbm.1, f32[12,2,512]{2,1,0:T(2,128)} %bitcast.1, bf16[2,1024,512]{2,1,0:T(8,128)(2,1)} %wq_hbm.1, ...), custom_call_target="tpu_custom_call" | custom-call | tf_op jit(solution)/shard_map/pallas_call | solution.py:533
  37.4 2.6 %shard_map.123 = (bf16[12,1024]{1,0:T(8,128)(2,1)}, f32[2,12,8,64,128]{4,3,2,1,0:T(8,128)}) custom-call(bf16[12,1024]{1,0:T(8,128)(2,1)S(1)} %get-tuple-element.4.hidden_ref, f32[2,12,8,64,128]{4,3,2,1,0:T(8,128)S(1)} %get-tuple-element.5.state_ref), custom_call_target="tpu_custom_call" | custom-call | tf_op jit(solution)/shard_map/pallas_call | solution.py:590

commit v4 on v3

--- a/solution.py
+++ b/solution.py
@@ -52,26 +52,20 @@
     return jnp.concatenate([upper, jnp.where(first_half(lower.shape), lower, 0.0)], axis=0)
 
 
-def stack_groups(blocks):
-    rows = []
-    for core in range(2):
-        one, two = blocks[core], blocks[2 + core]
-        upper_one = jnp.concatenate([one[:8, :256], one[8:, :256]], axis=1)
-        upper_two = jnp.concatenate([two[:8, :256], two[8:, :256]], axis=1)
-        lower = []
-        for half in range(2):
-            a, b = one[8 * half : 8 * half + 8, 256:], two[8 * half : 8 * half + 8, 256:]
-            top = first_half(a.shape)
-            lower += [jnp.where(top, a, swap(b)), jnp.where(top, swap(a), b)]
-        rows += [upper_one, upper_two, jnp.concatenate(lower, axis=1)]
-    return jnp.concatenate(rows, axis=0)
-
-
-def group_of(stacked, s):
-    chip, core = divmod(s, 2)
-    base = 24 * core
-    upper = stacked[base + 8 * chip : base + 8 * chip + 8]
-    return fold(upper, stacked[base + 16 : base + 24], chip)
+def stack_pair(one, two):
+    lower = []
+    for half in range(2):
+        a, b = one[8 * half : 8 * half + 8, 256:], two[8 * half : 8 * half + 8, 256:]
+        top = first_half(a.shape)
+        lower += [jnp.where(top, a, swap(b)), jnp.where(top, swap(a), b)]
+    return jnp.concatenate(
+        [
+            jnp.concatenate([one[:8, :256], one[8:, :256]], axis=1),
+            jnp.concatenate([two[:8, :256], two[8:, :256]], axis=1),
+            jnp.concatenate(lower, axis=1),
+        ],
+        axis=0,
+    )
 
 
 def block_kernel(
@@ -105,6 +99,7 @@
     other_chip = 1 - chip
     partner = 2 * chip + other_core
     across = 2 * other_chip + core
+    diagonal = 2 * other_chip + other_core
     mesh_id = pl.DeviceIdType.MESH
 
     barrier = pltpu.get_barrier_semaphore()
@@ -212,34 +207,46 @@
         def _():
             await_bytes(mix_recv.at[layer - 1], send_sem.at[0])
 
-    def send_mixed(layer, p):
+    def gated_pair(layer, half, which):
+        return stack_pair(
+            gated_all[layer, half, 2 * which].astype(F32),
+            gated_all[layer, half, 2 * which + 1].astype(F32),
+        ).astype(BF16)
+
+    def mix(layer, p, which, result):
         for k in range(2):
-
-            def send_to(owner):
-                remote(
-                    mix_send.at[layer, p, 2 * (owner - 1) + k],
-                    mix_recv.at[layer, p, k, tp - above],
-                    send_sem.at[5], mix_recv_sem.at[p, k], "tp", owner,
-                )
-
-            send_to(2 - above)
-
-            @pl.when(jnp.logical_not(is_owner))
+            group = 2 * which + k
+            mix_send[layer, p, group] = fold(
+                result[8 * k : 8 * k + 8], result[16:], k
+            ).astype(BF16)
+        for k in range(2):
+            group = 2 * which + k
+            if layer == layers - 1:
+                to = group
+                target = mix_last.at[p, lax.rem(tp - to + n_tp - 1, n_tp)]
+                arrival = mix_recv_sem.at[p, 0]
+            else:
+                to = 1 + which
+                target = mix_recv.at[layer, p, k, tp - above]
+                arrival = mix_recv_sem.at[p, k]
+
+            @pl.when(tp != to)
             def _():
-                send_to(1 + above)
-
-    lowest = tp == 0
-    last_order = (
-        jnp.where(lowest, 3, 0),
-        jnp.where(lowest, 2, 1 + lax.rem(tp, 3)),
-        jnp.where(lowest, 1, 1 + lax.rem(tp + 1, 3)),
-    )
-
-    def send_last(layer, p, to):
-        remote(
-            mix_send.at[layer, p, to], mix_last.at[p, lax.rem(tp - to + n_tp - 1, n_tp)],
-            send_sem.at[5], mix_recv_sem.at[p, 0], "tp", to,
-        )
+                remote(mix_send.at[layer, p, group], target, send_sem.at[5], arrival, "tp", to)
+
+    def renew(layer, begin, end):
+        for pair in range(begin, end):
+            adds = jnp.dot(fresh_columns[...], expand[0, pair], preferred_element_type=F32)
+            keeps = jnp.dot(fresh_columns[...], expand[1, pair], preferred_element_type=F32)
+            for k in range(2):
+                b = 2 * pair + k
+                lanes = slice(k * value_channels, (k + 1) * value_channels)
+                for h in range(heads):
+                    part = slice(h * head_key, (h + 1) * head_key)
+                    row = values[pl.ds(b, 1), pl.ds(h * value_channels, value_channels)]
+                    new_state_ref[layer, b, h] = (
+                        keeps[part, lanes] * state[layer, b, h] + adds[part, lanes] * row
+                    )
 
     def await_mixed_sends(layer):
         if layer == layers - 1:
@@ -327,7 +334,15 @@
         first, count = groups[0]
         for p in range(mix_pieces):
             await_features(layer, p)
-            widened = stack_groups([gathered[layer, p, s].astype(F32) for s in range(n_tp)])
+            widened = jnp.concatenate(
+                [
+                    stack_pair(
+                        gathered[layer, p, c].astype(F32), gathered[layer, p, 2 + c].astype(F32)
+                    )
+                    for c in range(2)
+                ],
+                axis=0,
+            )
             span = pl.ds(p * piece, piece)
             scaled.append((widened * gain[layer, span][None, :]).astype(BF16))
             for lane in range(0, piece, 128):
@@ -360,9 +375,13 @@
                     layer, i, jnp.dot(whole_rows, proj[layer, i], preferred_element_type=F32)
                 )
             send_group(layer, number)
-        pl.when(core != 0)(functools.partial(cross_first, layer))
-        for number in range(1, len(groups)):
-            cross_group(layer, number)
+            pl.when(core == 0)(functools.partial(cross_group, layer, number))
+
+        @pl.when(core != 0)
+        def _():
+            cross_first(layer)
+            for number in range(1, len(groups)):
+                cross_group(layer, number)
 
         await_bytes(sq_far.at[layer], sq_recv.at[1])
         chip_squares = sq_part[layer, core]
@@ -430,34 +449,26 @@
                 gated_heads.append(normed * (gate / (1.0 + jnp.exp(-gate))))
             gated = jnp.concatenate(gated_heads, axis=1)
             gated_all[layer, half, dp] = fold(gated[:8], gated[8:], 0).astype(BF16)
-            for j in range(1, n_dp):
-                remote(
-                    gated_all.at[layer, half, dp], gated_all.at[layer, half, dp],
-                    send_sem.at[4], gated_recv.at[half],
-                    "dp", lax.rem(dp + j, n_dp),
-                )
+            block = gated_all.at[layer, half, dp]
+            remote(block, block, send_sem.at[4], gated_recv.at[half], "dp", across)
+            remote(block, block, send_sem.at[4], gated_recv.at[half], "dp", diagonal)
+            remote(block, block, send_sem.at[4], gated_recv.at[halves], "dp", partner)
 
         fresh_columns[...] = columns_of(split(key) + split(decay))
-        for pair in range(rows // 2):
-            adds = jnp.dot(fresh_columns[...], expand[0, pair], preferred_element_type=F32)
-            keeps = jnp.dot(fresh_columns[...], expand[1, pair], preferred_element_type=F32)
-            for k in range(2):
-                b = 2 * pair + k
-                lanes = slice(k * value_channels, (k + 1) * value_channels)
-                for h in range(heads):
-                    part = slice(h * head_key, (h + 1) * head_key)
-                    row = values[pl.ds(b, 1), pl.ds(h * value_channels, value_channels)]
-                    new_state_ref[layer, b, h] = (
-                        keeps[part, lanes] * state[layer, b, h] + adds[part, lanes] * row
-                    )
+        first_pairs = rows // 4
+        renew(layer, 0, first_pairs)
 
         if layer == 0:
             await_bytes(wo, wo_sem)
+        await_bytes(gated_all.at[layer, :, pl.ds(0, 1)], gated_recv.at[halves])
+        gated = jnp.concatenate([gated_pair(layer, half, chip) for half in range(halves)], axis=1)
+        for p in range(mix_pieces):
+            columns = pl.ds(p * piece, piece)
+            mix(layer, p, chip, jnp.dot(gated, wo[layer, :, columns], preferred_element_type=F32))
+
         for half in range(halves):
-            await_bytes(gated_all.at[layer, half, pl.ds(0, n_dp - 1)], gated_recv.at[half])
-            gated = stack_groups(
-                [gated_all[layer, half, s].astype(F32) for s in range(n_dp)]
-            ).astype(BF16)
+            await_bytes(gated_all.at[layer, half, pl.ds(0, 2)], gated_recv.at[half])
+            gated = gated_pair(layer, half, other_chip)
             for p in range(mix_pieces):
                 columns = pl.ds(p * piece, piece)
                 result = jnp.dot(
@@ -468,18 +479,9 @@
                     result = result + mix_part[p]
                 if half < halves - 1:
                     mix_part[p] = result
-                    continue
-                for s in range(n_tp):
-                    mix_send[layer, p, s] = group_of(result, s).astype(BF16)
-                if layer < layers - 1:
-                    send_mixed(layer, p)
                 else:
-                    send_last(layer, p, last_order[0])
-
-        if layer == layers - 1:
-            for to in last_order[1:]:
-                for p in range(mix_pieces):
-                    send_last(layer, p, to)
+                    mix(layer, p, other_chip, result)
+        renew(layer, first_pairs, rows // 2)
 
         await_feature_sends(layer)
         await_bytes(sq_near.at[layer], send_sem.at[1])
@@ -564,7 +566,7 @@
             pltpu.VMEM((key_cols, 64), BF16),
             pltpu.VMEM((heads, 16, value_channels), F32),
             pltpu.VMEM((layers, halves, n_dp) + block, BF16),
-            pltpu.VMEM((mix_pieces, n_tp * rows, piece), F32),
+            pltpu.VMEM((mix_pieces, 2 * rows, piece), F32),
             pltpu.VMEM((layers, mix_pieces, n_tp) + block, BF16),
             pltpu.VMEM((layers - 1, mix_pieces, 2, n_tp - 1) + block, BF16),
             pltpu.VMEM((mix_pieces, n_tp - 1) + block, BF16),
@@ -576,7 +578,7 @@
             pltpu.SemaphoreType.DMA((1 + halves,)),
             pltpu.SemaphoreType.DMA((3 + halves,)),
             pltpu.SemaphoreType.DMA((2,)),
-            pltpu.SemaphoreType.DMA((halves,)),
+            pltpu.SemaphoreType.DMA((halves + 1,)),
             pltpu.SemaphoreType.DMA((mix_pieces, 2)),
             pltpu.SemaphoreType.DMA((7,)),
         ],

time: 40.2 us -> 38.9 us (0.968)
  Pallas kernels: 39.4 us -> 38.1 us
    pallas_call x1, Pallas kernels: 36.8 us -> 35.4 us  [fused(): pl.pallas_call(functools.partial(block_kernel, n_tp, n_dp, width * n_dp,...]
where the time goes in v4:
time: 38.9 us; the launch traced here: 38.7 us
  Pallas kernels  38.1 us (98%)
  between operations  0.64 us (2%)
    pallas_call x1, Pallas kernels, fused(): pl.pallas_call(functools.partial(block_kernel, n_tp, n_dp, width * n_dp,...  35.4 us
    pallas_call x1, Pallas kernels, fused(): pl.pallas_call(store_kernel, out_shape=(jax.ShapeDtypeStruct(hidden_in.sh...  2.62 us

profile of v4, /device:TPU:0, one launch (start us, length us, event | category | flops | bytes accessed | tf_op | source)
XLA Modules:
  0.0 38.7 jit_solution(8717494175479421740)
XLA Ops:
  0.6 35.4 %shard_map.122 = (bf16[12,1024]{1,0:T(8,128)(2,1)S(1)}, f32[2,12,8,64,128]{4,3,2,1,0:T(8,128)S(1)}) custom-call(bf16[12,1024]{1,0:T(8,128)(2,1)} %hidden_hbm.1, f32[2,1024]{1,0:T(2,128)} %gain_hbm.1, f32[2,1024]{1,0:T(2,128)} %out_gain_hbm.1, f32[12,2,512]{2,1,0:T(2,128)} %bitcast.1, bf16[2,1024,512]{2,1,0:T(8,128)(2,1)} %wq_hbm.1, ...), custom_call_target="tpu_custom_call" | custom-call | tf_op jit(solution)/shard_map/pallas_call | solution.py:535
  36.1 2.6 %shard_map.123 = (bf16[12,1024]{1,0:T(8,128)(2,1)}, f32[2,12,8,64,128]{4,3,2,1,0:T(8,128)}) custom-call(bf16[12,1024]{1,0:T(8,128)(2,1)S(1)} %get-tuple-element.4.hidden_ref, f32[2,12,8,64,128]{4,3,2,1,0:T(8,128)S(1)} %get-tuple-element.5.state_ref), custom_call_target="tpu_custom_call" | custom-call | tf_op jit(solution)/shard_map/pallas_call | solution.py:592

commit v5 on v4

--- a/solution.py
+++ b/solution.py
@@ -74,12 +74,12 @@
     wq_hbm, wk_hbm, wd_hbm, wv_hbm, wg_hbm, wo_hbm, state_hbm,
     hidden_out_ref, new_state_ref,
     hidden, gain, out_gain, offset, proj, wo, state,
-    gathered, product, partial, near, own, cross, far,
+    gathered, product, partial, near, own, cross, far, direct, far_direct,
     sq_part, sq_near, sq_cross, sq_far,
     expand, values, fresh_columns, readout,
     gated_all, mix_part, mix_send, mix_recv, mix_last,
     small_sem, proj_sem, wo_sem, state_sem,
-    gather_recv, near_recv, far_recv, sq_recv, gated_recv, mix_recv_sem, send_sem,
+    gather_recv, near_recv, far_recv, sq_recv, gated_recv, mix_recv_sem, direct_recv, send_sem,
 ):
     layers, rows, heads = state.shape[0], state.shape[1], state.shape[2]
     pad = 16
@@ -91,7 +91,6 @@
     half_heads = heads // halves
     pairs = tuple((3 + 2 * half, 2) for half in range(halves))
     groups = ((0, 3),) + pairs
-    parcels = ((0, 1), (1, 1), (2, 1)) + pairs
     tp = lax.axis_index("tp")
     dp = lax.axis_index("dp")
     chip, core = dp // 2, lax.rem(dp, 2)
@@ -136,6 +135,10 @@
     for copy in small:
         copy.start()
 
+    @pl.when(core == 0)
+    def _():
+        far_direct[...] = jnp.zeros_like(far_direct)
+
     row_of = lax.broadcasted_iota(jnp.int32, (4 * pad, 2 * value_channels), 0)
     lane_of = lax.broadcasted_iota(jnp.int32, (4 * pad, 2 * value_channels), 1)
     for second in range(2):
@@ -222,17 +225,47 @@
         for k in range(2):
             group = 2 * which + k
             if layer == layers - 1:
-                to = group
-                target = mix_last.at[p, lax.rem(tp - to + n_tp - 1, n_tp)]
-                arrival = mix_recv_sem.at[p, 0]
-            else:
-                to = 1 + which
-                target = mix_recv.at[layer, p, k, tp - above]
-                arrival = mix_recv_sem.at[p, k]
+                continue
+            to = 1 + which
 
             @pl.when(tp != to)
             def _():
-                remote(mix_send.at[layer, p, group], target, send_sem.at[5], arrival, "tp", to)
+                remote(
+                    mix_send.at[layer, p, group], mix_recv.at[layer, p, k, tp - above],
+                    send_sem.at[5], mix_recv_sem.at[p, k], "tp", to,
+                )
+
+    def send_last(layer, which):
+        for k in range(2):
+            to = 2 * which + k
+
+            @pl.when(tp != to)
+            def _():
+                for p in range(mix_pieces):
+                    remote(
+                        mix_send.at[layer, p, to],
+                        mix_last.at[p, lax.rem(tp - to + n_tp - 1, n_tp)],
+                        send_sem.at[5], mix_recv_sem.at[p, 0], "tp", to,
+                    )
+
+    def project_out(layer, which, arrivals, senders):
+        for half in range(halves):
+            await_bytes(
+                gated_all.at[layer, half, pl.ds(0, senders)], gated_recv.at[arrivals + half]
+            )
+            gated = gated_pair(layer, half, which)
+            for p in range(mix_pieces):
+                columns = pl.ds(p * piece, piece)
+                result = jnp.dot(
+                    gated, wo[layer, pl.ds(half * piece, piece), columns],
+                    preferred_element_type=F32,
+                )
+                if half > 0:
+                    result = result + mix_part[p]
+                if half < halves - 1:
+                    mix_part[p] = result
+                else:
+                    mix(layer, p, which, result)
 
     def renew(layer, begin, end):
         for pair in range(begin, end):
@@ -289,7 +322,29 @@
             send_sem.at[2], near_recv.at[number], "dp", partner,
         )
 
-    def cross_first(layer):
+    def halves_of(block):
+        tail = jnp.concatenate([block[:8, piece:], block[8:, piece:]], axis=1)
+        return block[:8, :piece], block[8:, :piece], tail
+
+    def of_other_chip(block):
+        zero, one, tail = halves_of(block)
+        return fold(jnp.where(chip == 0, one, zero), tail, other_chip).astype(BF16)
+
+    def of_this_chip(block):
+        zero, one, tail = halves_of(block)
+        return fold(jnp.where(chip == 0, zero, one), tail, chip)
+
+    def chip_sum(layer, i):
+        return partial[layer, core, i].astype(F32) + near[layer, i].astype(F32)
+
+    def send_cross(layer, number):
+        these = pl.ds(*groups[number])
+        remote(
+            cross.at[layer, these], far.at[layer, these],
+            send_sem.at[3], far_recv.at[number], "dp", across,
+        )
+
+    def cross_squares(layer):
         await_bytes(sq_near.at[layer], sq_recv.at[0])
         chip_squares = sq_part[layer, core] + sq_near[layer]
         sq_part[layer, core] = chip_squares
@@ -299,24 +354,44 @@
         remote(
             sq_cross.at[layer], sq_far.at[layer], send_sem.at[6], sq_recv.at[1], "dp", across
         )
-        cross_group(layer, 0)
+
+    def first_of_core_0(layer):
+        cross_squares(layer)
+        begin, amount = groups[0]
+        await_bytes(near.at[layer, pl.ds(begin, amount)], near_recv.at[0])
+        for i in range(begin, begin + amount):
+            cross[layer, i] = of_other_chip(chip_sum(layer, i))
+        send_cross(layer, 0)
+        for i in range(begin, begin + amount):
+            direct[layer, i] = of_other_chip(partial[layer, 1, i].astype(F32))
+        remote(
+            direct.at[layer], far_direct.at[layer],
+            send_sem.at[7], direct_recv, "dp", diagonal,
+        )
+        for i in range(begin, begin + amount):
+            own[i] = of_this_chip(chip_sum(layer, i))
+
+    def send_direct_of_core_1(layer):
+        begin, amount = groups[0]
+        for i in range(begin, begin + amount):
+            cross[layer, i] = of_other_chip(partial[layer, 1, i].astype(F32))
+        send_cross(layer, 0)
+
+    def first_of_core_1(layer):
+        cross_squares(layer)
+        begin, amount = groups[0]
+        await_bytes(near.at[layer, pl.ds(begin, amount)], near_recv.at[0])
+        for i in range(begin, begin + amount):
+            own[i] = of_this_chip(chip_sum(layer, i))
 
     def cross_group(layer, number):
         begin, amount = groups[number]
         await_bytes(near.at[layer, pl.ds(begin, amount)], near_recv.at[number])
         for i in range(begin, begin + amount):
-            both = partial[layer, core, i].astype(F32) + near[layer, i].astype(F32)
-            tail = jnp.concatenate([both[:8, piece:], both[8:, piece:]], axis=1)
-            zero, one = both[:8, :piece], both[8:, :piece]
-            cross[layer, i] = fold(jnp.where(chip == 0, one, zero), tail, other_chip).astype(BF16)
-            for parcel, (first, count) in enumerate(parcels):
-                if i == first + count - 1:
-                    these = pl.ds(first, count)
-                    remote(
-                        cross.at[layer, these], far.at[layer, these],
-                        send_sem.at[3], far_recv.at[parcel], "dp", across,
-                    )
-            own[i] = fold(jnp.where(chip == 0, zero, one), tail, chip)
+            cross[layer, i] = of_other_chip(chip_sum(layer, i))
+        send_cross(layer, number)
+        for i in range(begin, begin + amount):
+            own[i] = of_this_chip(chip_sum(layer, i))
 
     def split(block):
         high = block.astype(BF16).astype(F32)
@@ -366,7 +441,8 @@
                 else:
                     store_partial(layer, i, result)
         send_group(layer, 0)
-        pl.when(core == 0)(functools.partial(cross_first, layer))
+        pl.when(core == 0)(functools.partial(first_of_core_0, layer))
+        pl.when(core != 0)(functools.partial(send_direct_of_core_1, layer))
         whole_rows = jnp.concatenate(scaled, axis=1)
         for number in range(1, len(groups)):
             first, count = groups[number]
@@ -379,7 +455,7 @@
 
         @pl.when(core != 0)
         def _():
-            cross_first(layer)
+            first_of_core_1(layer)
             for number in range(1, len(groups)):
                 cross_group(layer, number)
 
@@ -397,13 +473,21 @@
         inverse = lax.rsqrt(jnp.sum(total_squares, axis=1, keepdims=True) / d_model + EPSILON)
 
         def projected(i):
-            for number, (first, count) in enumerate(parcels):
+            for number, (first, count) in enumerate(groups):
                 if i == first:
                     await_bytes(far.at[layer, pl.ds(first, count)], far_recv.at[number])
-            return unfold_rows(own[i] + far[layer, i].astype(F32)) * inverse
+            total = own[i] + far[layer, i].astype(F32)
+            if i < groups[0][1]:
+                total = total + far_direct[layer, i].astype(F32)
+            return unfold_rows(total) * inverse
 
         if layer == 0:
             await_bytes(state, state_sem)
+
+        @pl.when(core != 0)
+        def _():
+            await_bytes(far_direct.at[layer], direct_recv)
+
         logits = projected(0)
         log_sigmoid = jnp.minimum(logits, 0.0) - jnp.log(1.0 + jnp.exp(-jnp.abs(logits)))
         log_decay = log_sigmoid[:rows] / SOFTNESS + offset[:, layer, :]
@@ -452,7 +536,7 @@
             block = gated_all.at[layer, half, dp]
             remote(block, block, send_sem.at[4], gated_recv.at[half], "dp", across)
             remote(block, block, send_sem.at[4], gated_recv.at[half], "dp", diagonal)
-            remote(block, block, send_sem.at[4], gated_recv.at[halves], "dp", partner)
+            remote(block, block, send_sem.at[4], gated_recv.at[halves + half], "dp", partner)
 
         fresh_columns[...] = columns_of(split(key) + split(decay))
         first_pairs = rows // 4
@@ -460,27 +544,12 @@
 
         if layer == 0:
             await_bytes(wo, wo_sem)
-        await_bytes(gated_all.at[layer, :, pl.ds(0, 1)], gated_recv.at[halves])
-        gated = jnp.concatenate([gated_pair(layer, half, chip) for half in range(halves)], axis=1)
-        for p in range(mix_pieces):
-            columns = pl.ds(p * piece, piece)
-            mix(layer, p, chip, jnp.dot(gated, wo[layer, :, columns], preferred_element_type=F32))
-
-        for half in range(halves):
-            await_bytes(gated_all.at[layer, half, pl.ds(0, 2)], gated_recv.at[half])
-            gated = gated_pair(layer, half, other_chip)
-            for p in range(mix_pieces):
-                columns = pl.ds(p * piece, piece)
-                result = jnp.dot(
-                    gated, wo[layer, pl.ds(half * piece, piece), columns],
-                    preferred_element_type=F32,
-                )
-                if half > 0:
-                    result = result + mix_part[p]
-                if half < halves - 1:
-                    mix_part[p] = result
-                else:
-                    mix(layer, p, other_chip, result)
+        project_out(layer, chip, halves, 1)
+        if layer == layers - 1:
+            send_last(layer, chip)
+        project_out(layer, other_chip, 0, 2)
+        if layer == layers - 1:
+            send_last(layer, other_chip)
         renew(layer, first_pairs, rows // 2)
 
         await_feature_sends(layer)
@@ -488,6 +557,11 @@
         await_bytes(sq_far.at[layer], send_sem.at[6])
         await_bytes(near.at[layer], send_sem.at[2])
         await_bytes(far.at[layer], send_sem.at[3])
+
+        @pl.when(core == 0)
+        def _():
+            await_bytes(direct.at[layer], send_sem.at[7])
+
         await_bytes(gated_all.at[layer, :, pl.ds(0, n_dp - 1)], send_sem.at[4])
 
         if layer + 1 < layers:
@@ -557,6 +631,8 @@
             pltpu.VMEM((pieces,) + block, F32),
             pltpu.VMEM((layers, pieces) + block, BF16),
             pltpu.VMEM((layers, pieces) + block, BF16),
+            pltpu.VMEM((layers, 3) + block, BF16),
+            pltpu.VMEM((layers, 3) + block, BF16),
             pltpu.VMEM((layers, 2, 2 * rows, 128), F32),
             pltpu.VMEM((layers, 2 * rows, 128), F32),
             pltpu.VMEM((layers, 16, 128), F32),
@@ -576,11 +652,12 @@
             pltpu.SemaphoreType.DMA,
             pltpu.SemaphoreType.DMA((mix_pieces,)),
             pltpu.SemaphoreType.DMA((1 + halves,)),
-            pltpu.SemaphoreType.DMA((3 + halves,)),
+            pltpu.SemaphoreType.DMA((1 + halves,)),
             pltpu.SemaphoreType.DMA((2,)),
-            pltpu.SemaphoreType.DMA((halves + 1,)),
+            pltpu.SemaphoreType.DMA((2 * halves,)),
             pltpu.SemaphoreType.DMA((mix_pieces, 2)),
-            pltpu.SemaphoreType.DMA((7,)),
+            pltpu.SemaphoreType.DMA,
+            pltpu.SemaphoreType.DMA((8,)),
         ],
         compiler_params=pltpu.CompilerParams(
             collective_id=0, has_side_effects=True, vmem_limit_bytes=48 * 1024 * 1024

time: 38.9 us -> 38.7 us (level)
  no operation moved by 1% of the time
where the time goes in v5:
time: 38.7 us; the launch traced here: 38.5 us
  Pallas kernels  37.8 us (98%)
  between operations  0.64 us (2%)
    pallas_call x1, Pallas kernels, fused(): pl.pallas_call(functools.partial(block_kernel, n_tp, n_dp, width * n_dp,...  35.2 us
    pallas_call x1, Pallas kernels, fused(): pl.pallas_call(store_kernel, out_shape=(jax.ShapeDtypeStruct(hidden_in.sh...  2.62 us

profile of v5, /device:TPU:0, one launch (start us, length us, event | category | flops | bytes accessed | tf_op | source)
XLA Modules:
  0.0 38.5 jit_solution(11127684018874684137)
XLA Ops:
  0.6 35.2 %shard_map.122 = (bf16[12,1024]{1,0:T(8,128)(2,1)S(1)}, f32[2,12,8,64,128]{4,3,2,1,0:T(8,128)S(1)}) custom-call(bf16[12,1024]{1,0:T(8,128)(2,1)} %hidden_hbm.1, f32[2,1024]{1,0:T(2,128)} %gain_hbm.1, f32[2,1024]{1,0:T(2,128)} %out_gain_hbm.1, f32[12,2,512]{2,1,0:T(2,128)} %bitcast.1, bf16[2,1024,512]{2,1,0:T(8,128)(2,1)} %wq_hbm.1, ...), custom_call_target="tpu_custom_call" | custom-call | tf_op jit(solution)/shard_map/pallas_call | solution.py:609
  35.9 2.6 %shard_map.123 = (bf16[12,1024]{1,0:T(8,128)(2,1)}, f32[2,12,8,64,128]{4,3,2,1,0:T(8,128)}) custom-call(bf16[12,1024]{1,0:T(8,128)(2,1)S(1)} %get-tuple-element.4.hidden_ref, f32[2,12,8,64,128]{4,3,2,1,0:T(8,128)S(1)} %get-tuple-element.5.state_ref), custom_call_target="tpu_custom_call" | custom-call | tf_op jit(solution)/shard_map/pallas_call | solution.py:669

commit v6 on v5

--- a/solution.py
+++ b/solution.py
@@ -77,9 +77,9 @@
     gathered, product, partial, near, own, cross, far, direct, far_direct,
     sq_part, sq_near, sq_cross, sq_far,
     expand, values, fresh_columns, readout,
-    gated_all, mix_part, mix_send, mix_recv, mix_last,
+    gated_all, mix_part, mix_send, mix_recv, mix_other, mix_last, lent, handed,
     small_sem, proj_sem, wo_sem, state_sem,
-    gather_recv, near_recv, far_recv, sq_recv, gated_recv, mix_recv_sem, direct_recv, send_sem,
+    gather_recv, near_recv, far_recv, sq_recv, gated_recv, mix_recv_sem, direct_recv, lent_sem, send_sem,
 ):
     layers, rows, heads = state.shape[0], state.shape[1], state.shape[2]
     pad = 16
@@ -111,6 +111,12 @@
             barrier, inc=1, device_id={"dp": lax.rem(dp + j, n_dp)}, device_id_type=mesh_id
         )
 
+    for j in range(1, n_tp):
+        pl.semaphore_signal(
+            barrier, inc=1, device_id={"tp": lax.rem(tp + j, n_tp), "dp": partner},
+            device_id_type=mesh_id,
+        )
+
     small = [
         pltpu.make_async_copy(source, target, small_sem.at[index])
         for index, (source, target) in enumerate(
@@ -162,12 +168,15 @@
     for p in range(mix_pieces):
         span = slice(p * piece, (p + 1) * piece)
         gathered[0, p, tp] = fold(upper[:, span], lower[:, span], 0).astype(BF16)
-    pl.semaphore_wait(barrier, n_tp + n_dp - 2)
+    pl.semaphore_wait(barrier, 2 * n_tp + n_dp - 3)
 
     def remote(src, dst, send, recv, axis, target):
+        remote_to(src, dst, send, recv, {axis: target})
+
+    def remote_to(src, dst, send, recv, device):
         copy = pltpu.make_async_remote_copy(
             src_ref=src, dst_ref=dst, send_sem=send, recv_sem=recv,
-            device_id={axis: target}, device_id_type=mesh_id,
+            device_id=device, device_id_type=mesh_id,
         )
         copy.start()
 
@@ -175,7 +184,10 @@
         pltpu.make_async_copy(ref, ref, sem).wait()
 
     above = tp // 2
-    is_owner = (tp == 1) | (tp == 2)
+    middle = (tp == 1) | (tp == 2)
+    is_owner = middle & (core == 1)
+    lender = middle & (core == 0)
+    even_dp, odd_dp = 2 * chip, 2 * chip + 1
 
     def tp_step(j):
         return j + above * (n_tp - 2 * j)
@@ -209,6 +221,7 @@
         @pl.when(is_owner)
         def _():
             await_bytes(mix_recv.at[layer - 1], send_sem.at[0])
+            await_bytes(mix_other.at[layer - 1], send_sem.at[8])
 
     def gated_pair(layer, half, which):
         return stack_pair(
@@ -228,11 +241,18 @@
                 continue
             to = 1 + which
 
-            @pl.when(tp != to)
+            @pl.when((core == 1) & (tp != to))
             def _():
                 remote(
                     mix_send.at[layer, p, group], mix_recv.at[layer, p, k, tp - above],
-                    send_sem.at[5], mix_recv_sem.at[p, k], "tp", to,
+                    send_sem.at[5], mix_recv_sem.at[0, p, k], "tp", to,
+                )
+
+            @pl.when(core == 0)
+            def _():
+                remote_to(
+                    mix_send.at[layer, p, group], mix_other.at[layer, p, k, tp],
+                    send_sem.at[5], mix_recv_sem.at[1, p, k], {"tp": to, "dp": odd_dp},
                 )
 
     def send_last(layer, which):
@@ -245,7 +265,7 @@
                     remote(
                         mix_send.at[layer, p, to],
                         mix_last.at[p, lax.rem(tp - to + n_tp - 1, n_tp)],
-                        send_sem.at[5], mix_recv_sem.at[p, 0], "tp", to,
+                        send_sem.at[5], mix_recv_sem.at[0, p, 0], "tp", to,
                     )
 
     def project_out(layer, which, arrivals, senders):
@@ -294,20 +314,38 @@
         def _():
             await_bytes(mix_send.at[layer], send_sem.at[5])
 
+    def lend_residual(layer):
+        block = gathered.at[layer, :, pl.ds(2 * (tp - 1), 2)]
+        remote(block, lent.at[layer], send_sem.at[9], lent_sem, "dp", partner)
+
     def finish_middle(layer):
-        for p in range(mix_pieces):
-            for k in range(2):
-                await_bytes(mix_recv.at[layer, p, k], mix_recv_sem.at[p, k])
-                mine = 2 * (tp - 1) + k
-                total = mix_send[layer, p, mine].astype(F32)
-                for j in range(n_tp - 1):
-                    total = total + mix_recv[layer, p, k, j].astype(F32)
-                gathered[layer + 1, p, mine] = (
-                    gathered[layer, p, mine].astype(F32) + total
-                ).astype(BF16)
-                block = gathered.at[layer + 1, p, mine]
-                for to in (3 * (2 - tp), 3 - tp, 3 * (tp - 1)):
-                    remote(block, block, send_sem.at[0], gather_recv.at[p], "tp", to)
+        near_end, far_end = 3 * (tp - 1), 3 * (2 - tp)
+        units = [(p, k) for p in range(mix_pieces) for k in range(2)]
+        for p, k in units:
+            await_bytes(mix_recv.at[layer, p, k], mix_recv_sem.at[0, p, k])
+            mine = 2 * (tp - 1) + k
+            total = mix_send[layer, p, mine].astype(F32)
+            for j in range(n_tp - 1):
+                total = total + mix_recv[layer, p, k, j].astype(F32)
+            gathered[layer + 1, p, mine] = (
+                gathered[layer, p, mine].astype(F32) + total
+            ).astype(BF16)
+            block = gathered.at[layer + 1, p, mine]
+            for to in (far_end, 3 - tp, near_end):
+                remote(block, block, send_sem.at[0], gather_recv.at[p], "tp", to)
+        await_bytes(lent.at[layer], lent_sem)
+        for p, k in units:
+            await_bytes(mix_other.at[layer, p, k], mix_recv_sem.at[1, p, k])
+            mine = 2 * (tp - 1) + k
+            total = mix_other[layer, p, k, 0].astype(F32)
+            for j in range(1, n_tp):
+                total = total + mix_other[layer, p, k, j].astype(F32)
+            handed[layer, p, k] = (lent[layer, p, k].astype(F32) + total).astype(BF16)
+            for to in (far_end, 3 - tp, near_end, tp):
+                remote_to(
+                    handed.at[layer, p, k], gathered.at[layer + 1, p, mine],
+                    send_sem.at[8], gather_recv.at[p], {"tp": to, "dp": even_dp},
+                )
 
     def store_partial(layer, i, result):
         for c in range(2):
@@ -459,6 +497,8 @@
             for number in range(1, len(groups)):
                 cross_group(layer, number)
 
+        if layer + 1 < layers:
+            pl.when(lender)(functools.partial(lend_residual, layer))
         await_bytes(sq_far.at[layer], sq_recv.at[1])
         chip_squares = sq_part[layer, core]
         last = chip_squares[16:] + sq_far[layer, pl.ds(8, 8), :]
@@ -553,6 +593,12 @@
         renew(layer, first_pairs, rows // 2)
 
         await_feature_sends(layer)
+        if layer + 1 < layers:
+
+            @pl.when(lender)
+            def _():
+                await_bytes(lent.at[layer], send_sem.at[9])
+
         await_bytes(sq_near.at[layer], send_sem.at[1])
         await_bytes(sq_far.at[layer], send_sem.at[6])
         await_bytes(near.at[layer], send_sem.at[2])
@@ -568,7 +614,7 @@
             pl.when(is_owner)(functools.partial(finish_middle, layer))
         else:
             for p in range(mix_pieces):
-                await_bytes(mix_last.at[p], mix_recv_sem.at[p, 0])
+                await_bytes(mix_last.at[p], mix_recv_sem.at[0, p, 0])
                 total = mix_send[layer, p, tp].astype(F32)
                 for j in range(n_tp - 1):
                     total = total + mix_last[p, j].astype(F32)
@@ -645,7 +691,10 @@
             pltpu.VMEM((mix_pieces, 2 * rows, piece), F32),
             pltpu.VMEM((layers, mix_pieces, n_tp) + block, BF16),
             pltpu.VMEM((layers - 1, mix_pieces, 2, n_tp - 1) + block, BF16),
+            pltpu.VMEM((layers - 1, mix_pieces, 2, n_tp) + block, BF16),
             pltpu.VMEM((mix_pieces, n_tp - 1) + block, BF16),
+            pltpu.VMEM((layers - 1, mix_pieces, 2) + block, BF16),
+            pltpu.VMEM((layers - 1, mix_pieces, 2) + block, BF16),
             pltpu.SemaphoreType.DMA((4,)),
             pltpu.SemaphoreType.DMA((layers,)),
             pltpu.SemaphoreType.DMA,
@@ -655,9 +704,10 @@
             pltpu.SemaphoreType.DMA((1 + halves,)),
             pltpu.SemaphoreType.DMA((2,)),
             pltpu.SemaphoreType.DMA((2 * halves,)),
-            pltpu.SemaphoreType.DMA((mix_pieces, 2)),
+            pltpu.SemaphoreType.DMA((2, mix_pieces, 2)),
             pltpu.SemaphoreType.DMA,
-            pltpu.SemaphoreType.DMA((8,)),
+            pltpu.SemaphoreType.DMA,
+            pltpu.SemaphoreType.DMA((10,)),
         ],
         compiler_params=pltpu.CompilerParams(
             collective_id=0, has_side_effects=True, vmem_limit_bytes=48 * 1024 * 1024

time: 38.7 us -> 38.4 us (level)
  no operation moved by 1% of the time
where the time goes in v6:
time: 38.4 us; the launch traced here: 38.2 us
  Pallas kernels  37.6 us (98%)
  between operations  0.64 us (2%)
    pallas_call x1, Pallas kernels, fused(): pl.pallas_call(functools.partial(block_kernel, n_tp, n_dp, width * n_dp,...  35 us
    pallas_call x1, Pallas kernels, fused(): pl.pallas_call(store_kernel, out_shape=(jax.ShapeDtypeStruct(hidden_in.sh...  2.62 us

profile of v6, /device:TPU:0, one launch (start us, length us, event | category | flops | bytes accessed | tf_op | source)
XLA Modules:
  0.0 38.2 jit_solution(16632585732531040310)
XLA Ops:
  0.6 35.0 %shard_map.122 = (bf16[12,1024]{1,0:T(8,128)(2,1)S(1)}, f32[2,12,8,64,128]{4,3,2,1,0:T(8,128)S(1)}) custom-call(bf16[12,1024]{1,0:T(8,128)(2,1)} %hidden_hbm.1, f32[2,1024]{1,0:T(2,128)} %gain_hbm.1, f32[2,1024]{1,0:T(2,128)} %out_gain_hbm.1, f32[12,2,512]{2,1,0:T(2,128)} %bitcast.1, bf16[2,1024,512]{2,1,0:T(8,128)(2,1)} %wq_hbm.1, ...), custom_call_target="tpu_custom_call" | custom-call | tf_op jit(solution)/shard_map/pallas_call | solution.py:655
  35.6 2.6 %shard_map.123 = (bf16[12,1024]{1,0:T(8,128)(2,1)}, f32[2,12,8,64,128]{4,3,2,1,0:T(8,128)}) custom-call(bf16[12,1024]{1,0:T(8,128)(2,1)S(1)} %get-tuple-element.4.hidden_ref, f32[2,12,8,64,128]{4,3,2,1,0:T(8,128)S(1)} %get-tuple-element.5.state_ref), custom_call_target="tpu_custom_call" | custom-call | tf_op jit(solution)/shard_map/pallas_call | solution.py:719

commit v7 on v6

--- a/solution.py
+++ b/solution.py
@@ -221,7 +221,7 @@
         @pl.when(is_owner)
         def _():
             await_bytes(mix_recv.at[layer - 1], send_sem.at[0])
-            await_bytes(mix_other.at[layer - 1], send_sem.at[8])
+            await_bytes(mix_other.at[layer - 1], send_sem.at[5])
 
     def gated_pair(layer, half, which):
         return stack_pair(
@@ -245,14 +245,14 @@
             def _():
                 remote(
                     mix_send.at[layer, p, group], mix_recv.at[layer, p, k, tp - above],
-                    send_sem.at[5], mix_recv_sem.at[0, p, k], "tp", to,
+                    send_sem.at[2], mix_recv_sem.at[0, p, k], "tp", to,
                 )
 
             @pl.when(core == 0)
             def _():
                 remote_to(
                     mix_send.at[layer, p, group], mix_other.at[layer, p, k, tp],
-                    send_sem.at[5], mix_recv_sem.at[1, p, k], {"tp": to, "dp": odd_dp},
+                    send_sem.at[2], mix_recv_sem.at[1, p, k], {"tp": to, "dp": odd_dp},
                 )
 
     def send_last(layer, which):
@@ -265,7 +265,7 @@
                     remote(
                         mix_send.at[layer, p, to],
                         mix_last.at[p, lax.rem(tp - to + n_tp - 1, n_tp)],
-                        send_sem.at[5], mix_recv_sem.at[0, p, 0], "tp", to,
+                        send_sem.at[2], mix_recv_sem.at[0, p, 0], "tp", to,
                     )
 
     def project_out(layer, which, arrivals, senders):
@@ -303,20 +303,20 @@
 
     def await_mixed_sends(layer):
         if layer == layers - 1:
-            await_bytes(mix_last, send_sem.at[5])
+            await_bytes(mix_last, send_sem.at[2])
             return
 
         @pl.when(is_owner)
         def _():
-            await_bytes(mix_send.at[layer, :, pl.ds(0, 2)], send_sem.at[5])
+            await_bytes(mix_send.at[layer, :, pl.ds(0, 2)], send_sem.at[2])
 
         @pl.when(jnp.logical_not(is_owner))
         def _():
-            await_bytes(mix_send.at[layer], send_sem.at[5])
+            await_bytes(mix_send.at[layer], send_sem.at[2])
 
     def lend_residual(layer):
         block = gathered.at[layer, :, pl.ds(2 * (tp - 1), 2)]
-        remote(block, lent.at[layer], send_sem.at[9], lent_sem, "dp", partner)
+        remote(block, lent.at[layer], send_sem.at[6], lent_sem, "dp", partner)
 
     def finish_middle(layer):
         near_end, far_end = 3 * (tp - 1), 3 * (2 - tp)
@@ -344,7 +344,7 @@
             for to in (far_end, 3 - tp, near_end, tp):
                 remote_to(
                     handed.at[layer, p, k], gathered.at[layer + 1, p, mine],
-                    send_sem.at[8], gather_recv.at[p], {"tp": to, "dp": even_dp},
+                    send_sem.at[5], gather_recv.at[p], {"tp": to, "dp": even_dp},
                 )
 
     def store_partial(layer, i, result):
@@ -357,7 +357,7 @@
         these = pl.ds(*groups[number])
         remote(
             partial.at[layer, other_core, these], near.at[layer, these],
-            send_sem.at[2], near_recv.at[number], "dp", partner,
+            send_sem.at[1], near_recv.at[number], "dp", partner,
         )
 
     def halves_of(block):
@@ -379,7 +379,7 @@
         these = pl.ds(*groups[number])
         remote(
             cross.at[layer, these], far.at[layer, these],
-            send_sem.at[3], far_recv.at[number], "dp", across,
+            send_sem.at[1], far_recv.at[number], "dp", across,
         )
 
     def cross_squares(layer):
@@ -390,7 +390,7 @@
             [jnp.where(chip == 0, chip_squares[8:16], chip_squares[:8]), chip_squares[16:]], axis=0
         )
         remote(
-            sq_cross.at[layer], sq_far.at[layer], send_sem.at[6], sq_recv.at[1], "dp", across
+            sq_cross.at[layer], sq_far.at[layer], send_sem.at[3], sq_recv.at[1], "dp", across
         )
 
     def first_of_core_0(layer):
@@ -404,7 +404,7 @@
             direct[layer, i] = of_other_chip(partial[layer, 1, i].astype(F32))
         remote(
             direct.at[layer], far_direct.at[layer],
-            send_sem.at[7], direct_recv, "dp", diagonal,
+            send_sem.at[4], direct_recv, "dp", diagonal,
         )
         for i in range(begin, begin + amount):
             own[i] = of_this_chip(chip_sum(layer, i))
@@ -541,8 +541,7 @@
             for h in range(heads)
         ]
 
-        for half in range(halves):
-            base = half * half_heads
+        for base in range(0, heads, half_heads):
             columns = read_columns[base * head_key : (base + half_heads) * head_key]
             for pair in range(rows // 2):
                 factors = jnp.dot(
@@ -558,6 +557,9 @@
                         readout[base + hh, pl.ds(b, 1), :] = jnp.sum(
                             factor * state[layer, b, base + hh], axis=0, keepdims=True
                         )
+
+        for half in range(halves):
+            base = half * half_heads
             value = projected(3 + 2 * half)
             gate_all = projected(4 + 2 * half)
             values[:, pl.ds(half * piece, piece)] = value
@@ -574,9 +576,9 @@
             gated = jnp.concatenate(gated_heads, axis=1)
             gated_all[layer, half, dp] = fold(gated[:8], gated[8:], 0).astype(BF16)
             block = gated_all.at[layer, half, dp]
-            remote(block, block, send_sem.at[4], gated_recv.at[half], "dp", across)
-            remote(block, block, send_sem.at[4], gated_recv.at[half], "dp", diagonal)
-            remote(block, block, send_sem.at[4], gated_recv.at[halves + half], "dp", partner)
+            remote(block, block, send_sem.at[1], gated_recv.at[half], "dp", across)
+            remote(block, block, send_sem.at[1], gated_recv.at[half], "dp", diagonal)
+            remote(block, block, send_sem.at[1], gated_recv.at[halves + half], "dp", partner)
 
         fresh_columns[...] = columns_of(split(key) + split(decay))
         first_pairs = rows // 4
@@ -597,18 +599,15 @@
 
             @pl.when(lender)
             def _():
-                await_bytes(lent.at[layer], send_sem.at[9])
-
-        await_bytes(sq_near.at[layer], send_sem.at[1])
-        await_bytes(sq_far.at[layer], send_sem.at[6])
-        await_bytes(near.at[layer], send_sem.at[2])
-        await_bytes(far.at[layer], send_sem.at[3])
+                await_bytes(lent.at[layer], send_sem.at[6])
+
+        await_bytes(sq_far.at[layer], send_sem.at[3])
+        await_bytes(partial.at[layer], send_sem.at[1])
 
         @pl.when(core == 0)
         def _():
-            await_bytes(direct.at[layer], send_sem.at[7])
-
-        await_bytes(gated_all.at[layer, :, pl.ds(0, n_dp - 1)], send_sem.at[4])
+            await_bytes(direct.at[layer], send_sem.at[4])
+
 
         if layer + 1 < layers:
             pl.when(is_owner)(functools.partial(finish_middle, layer))
@@ -707,7 +706,7 @@
             pltpu.SemaphoreType.DMA((2, mix_pieces, 2)),
             pltpu.SemaphoreType.DMA,
             pltpu.SemaphoreType.DMA,
-            pltpu.SemaphoreType.DMA((10,)),
+            pltpu.SemaphoreType.DMA((7,)),
         ],
         compiler_params=pltpu.CompilerParams(
             collective_id=0, has_side_effects=True, vmem_limit_bytes=48 * 1024 * 1024

time: 38.4 us -> 38.3 us (level)
  no operation moved by 1% of the time
where the time goes in v7:
time: 38.3 us; the launch traced here: 38.2 us
  Pallas kernels  37.5 us (98%)
  between operations  0.64 us (2%)
    pallas_call x1, Pallas kernels, fused(): pl.pallas_call(functools.partial(block_kernel, n_tp, n_dp, width * n_dp,...  34.9 us
    pallas_call x1, Pallas kernels, fused(): pl.pallas_call(store_kernel, out_shape=(jax.ShapeDtypeStruct(hidden_in.sh...  2.62 us

profile of v7, /device:TPU:0, one launch (start us, length us, event | category | flops | bytes accessed | tf_op | source)
XLA Modules:
  0.0 38.2 jit_solution(14877032156809260428)
XLA Ops:
  0.6 34.9 %shard_map.122 = (bf16[12,1024]{1,0:T(8,128)(2,1)S(1)}, f32[2,12,8,64,128]{4,3,2,1,0:T(8,128)S(1)}) custom-call(bf16[12,1024]{1,0:T(8,128)(2,1)} %hidden_hbm.1, f32[2,1024]{1,0:T(2,128)} %gain_hbm.1, f32[2,1024]{1,0:T(2,128)} %out_gain_hbm.1, f32[12,2,512]{2,1,0:T(2,128)} %bitcast.1, bf16[2,1024,512]{2,1,0:T(8,128)(2,1)} %wq_hbm.1, ...), custom_call_target="tpu_custom_call" | custom-call | tf_op jit(solution)/shard_map/pallas_call | solution.py:654
  35.5 2.6 %shard_map.123 = (bf16[12,1024]{1,0:T(8,128)(2,1)}, f32[2,12,8,64,128]{4,3,2,1,0:T(8,128)}) custom-call(bf16[12,1024]{1,0:T(8,128)(2,1)S(1)} %get-tuple-element.4.hidden_ref, f32[2,12,8,64,128]{4,3,2,1,0:T(8,128)S(1)} %get-tuple-element.5.state_ref), custom_call_target="tpu_custom_call" | custom-call | tf_op jit(solution)/shard_map/pallas_call | solution.py:718
